TPU v7x, 512 devices: a whole 4x8x8 slice. The times are simulated.
512 devices in a mesh: sp: 32 (over z, x), tp: 16 (over y, core).
Axes of the slice: x: 4, y: 8, z: 8, core: 2. Of those that a mesh axis runs over, the one named last changes fastest.
Arguments:
- query_matrix: bfloat16 [8192, 1024], P('sp', 'tp'), may hold values from -6 to 6
- key_matrix: bfloat16 [8192, 1024], P('sp', 'tp'), may hold values from -6 to 6
- value_matrix: bfloat16 [8192, 2048], P('sp', 'tp'), may hold values from -6 to 6
- output_gate_rows: bfloat16 [8192, 2048], P('sp', 'tp'), may hold values from -6 to 6
- decay_preactivation: bfloat16 [8192, 1024], P('sp', 'tp'), may hold values from -5 to 5
- channel_decay_bias: float32 [1024], P('tp'), may hold values from 0 to 10
- extra_log_decay: float32 [8192, 16], P('sp', 'tp'), may hold values from -0.7 to 0
- head_norm_gain: float32 [128], replicated, may hold values from 0.1 to 1.9
- output_projection: bfloat16 [2048, 2048], P('tp'), may hold values from -0.125 to 0.125
- residual_input: bfloat16 [8192, 2048], P(('sp', 'tp')), may hold values from -6 to 6
- attention_norm_gain: float32 [2048], replicated, may hold values from 0.1 to 1.9
- expert_before_gain: float32 [2048], replicated, may hold values from 0.1 to 1.9
- expert_after_gain: float32 [2048], replicated, may hold values from 0.1 to 1.9
- expert_gate_weight: bfloat16 [32, 2048, 4096], P('sp', None, 'tp'), may hold values from -0.125 to 0.125
- expert_up_weight: bfloat16 [32, 2048, 4096], P('sp', None, 'tp'), may hold values from -0.125 to 0.125
- expert_down_weight: bfloat16 [32, 4096, 2048], P('sp', 'tp'), may hold values from -0.09375 to 0.09375
- token_expert_index: int32 [8192, 2], P('sp'), may hold values from 0 to 31, as said below
- routing_weight_matrix: float32 [8192, 2], P('sp'), may hold values from 0.1 to 1
Outputs:
- layer_out: bfloat16 [8192, 2048], P(('sp', 'tp'))
Inputs may be any that keep to these rules, and one draw needn't show every extreme that they name: `token_expert_index`: the 2 experts of a token differ and lie in one group: they have the same value of e // 4. In each aligned block of 256 rows (the rows of one index of sp) no expert is named by more than 20 rows, and the 4 experts of one group are each named by exactly 20 rows in every block.
All inputs are finite; a program needn't handle non-finite values.
Results may differ from a plain program's by a relative error of at most 0.024.
Values may be sent and summed in bfloat16 or wider, within the bound.
A program may use at most 64 MiB of HBM per device.

v0:
```python
import jax
import jax.numpy as jnp
from jax import lax
from jax.sharding import PartitionSpec as P

KEY_CHANNELS = 64
DV = 128
TOP = 2
BLOCK = 64


EPSILON = 1e-06
DECAY_NORMALIZER = 16.0
HIGHEST = lax.Precision.HIGHEST


def copy_for_each(shard, axis):
    peers = lax.axis_size(axis)
    return lax.all_to_all(
        jnp.broadcast_to(shard[None], (peers, *shard.shape)), axis, 0, 0, tiled=True
    )


def gathered_once(shard, axis):
    leaves = jax.tree.leaves(shard)
    turns = sorted(range(len(leaves)), key=lambda k: -leaves[k].size)
    width = (1, *leaves[turns[0]].shape)[-1]
    lines = [
        jnp.pad(leaves[k].reshape(-1), (0, -leaves[k].size % width)).reshape(-1, width)
        for k in turns
    ]
    both, at, found = (copy_for_each(jnp.concatenate(lines), axis), 0, {})
    for k, line in zip(turns, lines):
        section = both[:, at : at + len(line)].reshape(len(both), -1)
        found[k] = section[:, : leaves[k].size].reshape(-1, *leaves[k].shape)
        at += len(line)
    numbers = iter(range(len(leaves)))
    return jax.tree.map(lambda _: found[next(numbers)], shard)


def combined_pairwise(pieces, combine):
    while len(jax.tree.leaves(pieces)[0]) > 1:
        pieces = jax.vmap(combine)(
            *(jax.tree.map(lambda part: part[side::2], pieces) for side in (0, 1))
        )
    return jax.tree.map(lambda part: part[0], pieces)


def carried_in(shard, axis, combine, identity):
    peers, position = (lax.axis_size(axis), lax.axis_index(axis))
    passed = jnp.arange(peers) < position

    def kept(part, zero, own):
        part = jnp.where(
            passed.reshape(-1, *(1 for _ in own.shape)),
            part.astype(own.dtype),
            jnp.asarray(zero, own.dtype),
        )
        return part

    pieces = gathered_once(
        jax.tree.map(lambda part, kind: part.astype(kind), shard, (jnp.bfloat16, jnp.bfloat16)),
        axis,
    )
    return combined_pairwise(jax.tree.map(kept, pieces, identity, shard), combine)


def split_up(shard, dim, peers):
    shape = shard.shape
    parts = shard.reshape(*shape[:dim], peers, shape[dim] // peers, *shape[dim + 1 :])
    return jnp.moveaxis(parts, dim, 0)


def sum_at_owner(shard, axis, dim):
    peers = lax.axis_size(axis)
    parts = lax.all_to_all(split_up(shard, dim, peers), axis, 0, 0, tiled=True)
    return jnp.sum(parts.astype(jnp.float32), axis=0)


def laid_out(parts, dim):
    parts = jnp.moveaxis(parts, 0, dim)
    shape = parts.shape
    return parts.reshape(*shape[:dim], shape[dim] * shape[dim + 1], *shape[dim + 2 :])


def collect(shard, axis, dim):
    return laid_out(copy_for_each(shard, axis), dim)


def rms_scale(values, gain_row):
    return (
        values * lax.rsqrt(jnp.mean(values * values, axis=-1, keepdims=True) + EPSILON) * gain_row
    )


def join_states(earlier, later):
    fade_one, state_one = earlier
    fade_two, state_two = later
    return (fade_one * fade_two, fade_two[..., None] * state_one + state_two)


def advance(running_state, inputs_pair):
    fade_now, grow_now = inputs_pair
    return (fade_now[..., None] * running_state + grow_now, running_state)


def shards(
    query_matrix,
    key_matrix,
    value_matrix,
    output_gate_rows,
    decay_preactivation,
    channel_decay_bias,
    extra_log_decay,
    head_norm_gain,
    output_projection,
    residual_input,
    attention_norm_gain,
    expert_before_gain,
    expert_after_gain,
    expert_gate_weight,
    expert_up_weight,
    expert_down_weight,
    token_expert_index,
    routing_weight_matrix,
):
    sequence_length = query_matrix.shape[0]
    number_heads = value_matrix.shape[1] // DV
    blocks = sequence_length // BLOCK
    queries = query_matrix.astype(jnp.float32).reshape(
        sequence_length, number_heads, KEY_CHANNELS
    ) * KEY_CHANNELS ** (-0.5)
    keys_all = key_matrix.astype(jnp.float32).reshape(sequence_length, number_heads, KEY_CHANNELS)
    values_all = value_matrix.astype(jnp.float32).reshape(sequence_length, number_heads, DV)
    decay_logarithm = (
        jax.nn.log_sigmoid(decay_preactivation.astype(jnp.float32) + channel_decay_bias)
        / DECAY_NORMALIZER
    )
    decay_logarithm = (
        decay_logarithm.reshape(sequence_length, number_heads, KEY_CHANNELS)
        + extra_log_decay[:, :, None]
    )
    running = jnp.cumsum(decay_logarithm, axis=0)
    total_fade = jnp.exp(running[-1])
    keys_to_end = keys_all * jnp.exp(running[-1] - running)
    total_growth = jnp.einsum("thd,thv->hdv", keys_to_end, values_all, precision=HIGHEST)
    q_blocks = queries.reshape(blocks, BLOCK, number_heads, KEY_CHANNELS)
    k_blocks = keys_all.reshape(blocks, BLOCK, number_heads, KEY_CHANNELS)
    v_blocks = values_all.reshape(blocks, BLOCK, number_heads, DV)
    inside = jnp.cumsum(decay_logarithm.reshape(blocks, BLOCK, number_heads, KEY_CHANNELS), axis=1)
    block_end = inside[:, -1:]
    q_decayed = q_blocks * jnp.exp(inside)
    k_inverse = k_blocks * jnp.exp(-inside)
    k_to_end = k_blocks * jnp.exp(block_end - inside)
    causal = jnp.tril(jnp.ones((BLOCK, BLOCK), dtype=bool))
    scores = jnp.einsum("nihd,njhd->nhij", q_decayed, k_inverse, precision=HIGHEST)
    scores = jnp.where(causal, scores, 0.0)
    within = jnp.einsum("nhij,njhv->nihv", scores, v_blocks, precision=HIGHEST)
    growth = jnp.einsum("nchd,nchv->nhdv", k_to_end, v_blocks, precision=HIGHEST)
    fade_rows = jnp.exp(block_end[:, 0])
    identity = (jnp.ones_like(total_fade), jnp.zeros_like(total_growth))
    _, carried = carried_in((total_fade, total_growth), "sp", join_states, identity)
    _, starts = lax.scan(advance, carried, (fade_rows, growth))
    across = jnp.einsum("nchd,nhdv->nchv", q_decayed, starts, precision=HIGHEST)
    attn = (within + across).reshape(sequence_length, number_heads, DV)
    gate_act = jax.nn.silu(
        output_gate_rows.astype(jnp.float32).reshape(sequence_length, number_heads, DV)
    )
    gated = (
        (rms_scale(attn, head_norm_gain) * gate_act)
        .astype(jnp.bfloat16)
        .reshape(sequence_length, number_heads * DV)
    )
    mixed = sum_at_owner(
        jnp.dot(gated, output_projection, preferred_element_type=jnp.float32).astype(jnp.bfloat16),
        "tp",
        0,
    )
    layer_mid = (residual_input.astype(jnp.float32) + rms_scale(mixed, attention_norm_gain)).astype(
        jnp.bfloat16
    )
    normed = rms_scale(layer_mid.astype(jnp.float32), expert_before_gain).astype(jnp.bfloat16)
    block_rows = collect(normed, "tp", 0)
    expert_count = lax.axis_size("sp")
    capacity = 5 * sequence_length // (2 * expert_count)
    flat_ids = token_expert_index.reshape(sequence_length * TOP)
    one_hot = (flat_ids[:, None] == jnp.arange(expert_count, dtype=jnp.int32)[None, :]).astype(
        jnp.int32
    )
    slot_index = jnp.sum((jnp.cumsum(one_hot, axis=0) - one_hot) * one_hot, axis=1)
    target = flat_ids * capacity + slot_index
    owners = jnp.zeros((expert_count * capacity,), jnp.int32)
    owners = owners.at[target].set(jnp.arange(sequence_length * TOP, dtype=jnp.int32) // TOP)
    owners = owners.reshape(expert_count, capacity)
    outgoing = block_rows[owners]
    arrived = lax.all_to_all(outgoing, "sp", split_axis=0, concat_axis=0, tiled=True)
    sources, slot_count, col_count = arrived.shape
    rows_in = arrived.reshape(sources * slot_count, col_count)
    gate_part = jnp.dot(rows_in, expert_gate_weight[0], preferred_element_type=jnp.float32)
    up_part = jnp.dot(rows_in, expert_up_weight[0], preferred_element_type=jnp.float32)
    hidden = (jax.nn.silu(gate_part) * up_part).astype(jnp.bfloat16)
    partial_value = jnp.dot(hidden, expert_down_weight[0], preferred_element_type=jnp.float32)
    partial_value = partial_value.reshape(sources, slot_count, col_count)
    share_part = sum_at_owner(partial_value.astype(jnp.bfloat16), "tp", 2).astype(jnp.bfloat16)
    back_rows = lax.all_to_all(share_part, "sp", split_axis=0, concat_axis=0, tiled=True)
    lookup = back_rows.reshape(expert_count * capacity, back_rows.shape[2])
    token_target = target.reshape(sequence_length, TOP)
    picked = lookup[token_target].astype(jnp.float32)
    column_sums = jnp.sum(routing_weight_matrix[:, :, None] * picked, axis=1)
    branch = lax.all_to_all(
        column_sums.astype(jnp.bfloat16), "tp", split_axis=0, concat_axis=1, tiled=True
    ).astype(column_sums.dtype)
    return (layer_mid.astype(jnp.float32) + rms_scale(branch, expert_after_gain)).astype(
        jnp.bfloat16
    )


def solution(mesh):
    placed = (
        P("sp", "tp"),
        P("sp", "tp"),
        P("sp", "tp"),
        P("sp", "tp"),
        P("sp", "tp"),
        P("tp"),
        P("sp", "tp"),
        P(),
        P("tp", None),
        P(("sp", "tp"), None),
        P(),
        P(),
        P(),
        P("sp", None, "tp"),
        P("sp", None, "tp"),
        P("sp", "tp", None),
        P("sp", None),
        P("sp", None),
    )
    return jax.shard_map(
        shards, mesh=mesh, in_specs=placed, out_specs=P(("sp", "tp"), None), check_vma=False
    )
```

profile of v0, /device:TPU:1, one launch (start us, length us, event | category | flops | bytes accessed | tf_op | source)
XLA Modules:
  0.0 307.7 jit_solution(7750839254290669792)
XLA Ops:
  0.0 1.0 fusion.33
  1.0 0.6 reduce-window.14
  1.6 0.2 slice_reduce_fusion.1
  1.9 0.1 copy.93
  2.0 0.1 broadcast.174
  2.2 0.9 slice_reduce_fusion.2
  3.2 0.8 convert_element_type.100
  4.0 0.2 exponential_multiply_fusion.3
  4.1 1.0 convolution_convert_fusion.2
  5.2 0.9 broadcast_in_dim.52
  6.0 13.7 %all-to-all-start = ((bf16[32,65,128]{2,1,0:T(8,128)(2,1)}), bf16[32,65,128]{2,1,0:T(8,128)(2,1)S(1)}, u32[]{:S(2)}, u32[]{:S(2)}) async-start(bf16[32,65,128]{2,1,0:T(8,128)(2,1)} %broadcast_in_dim.52), calls=%async_computation | async-start | bytes 1179648 | tf_op jit(solution)/shard_map/all_to_all | solution.py:19
  19.8 0.1 copy.90
  20.0 0.1 copy.88
  20.1 0.1 fusion.49
  20.3 0.3 convolution_bitcast_fusion
  20.6 0.4 convolution_select_fusion
  20.9 16.4 %all-to-all-done = bf16[32,65,128]{2,1,0:T(8,128)(2,1)S(1)} async-done(((bf16[32,65,128]{2,1,0:T(8,128)(2,1)}), bf16[32,65,128]{2,1,0:T(8,128)(2,1)S(1)}, u32[]{:S(2)}, u32[]{:S(2)}) %all-to-all-start) | async-done | bytes 532512 | tf_op jit(solution)/shard_map/all_to_all | solution.py:19
  37.6 0.1 select_bitcast_fusion
  37.8 0.2 slice_add_fusion
  38.0 0.1 slice_add_fusion.1
  38.2 0.1 slice_add_fusion.2
  38.4 0.4 while.12
  38.9 0.3 fusion.22
  39.1 0.3 fusion.21
  39.5 0.1 fusion.30
  39.7 0.4 convolution_convert_fusion.1
  40.1 37.7 %all_to_all.40 = bf16[16,16,2048]{2,1,0:T(8,128)(2,1)S(1)} all-to-all(bf16[16,16,2048]{2,1,0:T(8,128)(2,1)S(1)} %bitcast.152), channel_id=1, replica_groups=mesh['sp'=32,'tp'=16] {'tp'}, dimensions={0} | all-to-all | bytes 2097152 | tf_op jit(solution)/shard_map/all_to_all | solution.py:76
  77.8 0.1 convert_reduce_fusion
  78.0 0.1 multiply_reduce_fusion
  78.1 0.2 fusion.15
  78.4 1.1 broadcast_in_dim.57
  79.5 3.5 %all-to-all-start.2 = ((bf16[16,16,2048]{2,1,0:T(8,128)(2,1)}), bf16[16,16,2048]{2,1,0:T(8,128)(2,1)S(1)}, u32[]{:S(2)}, u32[]{:S(2)}) async-start(bf16[16,16,2048]{2,1,0:T(8,128)(2,1)} %broadcast_in_dim.57), calls=%async_computation.2 | async-start | bytes 2097152 | tf_op jit(solution)/shard_map/all_to_all | solution.py:19
  83.1 0.1 copy.99
  83.3 0.1 eq.29
  83.4 0.1 eq.25
  83.6 1.2 reduce-window.16
  84.7 0.2 slice_reduce_fusion
  85.0 0.1 fusion.36
  85.1 0.1 reduce_sum.86
  85.3 0.1 mul.273
  85.5 2.4 scatter_custom_fusion
  87.9 0.1 reshape.376
  88.0 0.1 reshape.383
  88.1 22.3 %all-to-all-done.2 = bf16[16,16,2048]{2,1,0:T(8,128)(2,1)S(1)} async-done(((bf16[16,16,2048]{2,1,0:T(8,128)(2,1)}), bf16[16,16,2048]{2,1,0:T(8,128)(2,1)S(1)}, u32[]{:S(2)}, u32[]{:S(2)}) %all-to-all-start.2) | async-done | bytes 1048608 | tf_op jit(solution)/shard_map/all_to_all | solution.py:19
  110.5 4.1 %gather_fusion = bf16[640,2048]{1,0:T(8,128)(2,1)} fusion(bf16[256,2048]{1,0:T(8,128)(2,1)S(1)} %bitcast.150, s32[1024]{0:T(1024)S(1)} %pad_clamp_fusion.1), kind=kCustom, calls=%fused_computation | custom fusion | bytes 5245440 | tf_op jit(solution)/shard_map/gather | solution.py:195
  114.5 5.2 %reshape.382 = bf16[32,20,2048]{2,1,0:T(8,128)(2,1)} reshape(bf16[640,2048]{1,0:T(8,128)(2,1)} %gather_fusion) | data formatting | bytes 5242880 | tf_op jit(solution)/shard_map/gather | solution.py:195
  119.7 77.0 %all_to_all.41 = bf16[32,20,2048]{2,1,0:T(8,128)(2,1)} all-to-all(bf16[32,20,2048]{2,1,0:T(8,128)(2,1)} %reshape.382), channel_id=1, replica_groups=mesh['sp'=32,'tp'=16] {'sp'}, dimensions={0} | all-to-all | bytes 5242880 | tf_op jit(solution)/shard_map/all_to_all | solution.py:196
  196.7 5.3 %reshape.377 = bf16[640,2048]{1,0:T(8,128)(2,1)} reshape(bf16[32,20,2048]{2,1,0:T(8,128)(2,1)} %all_to_all.41) | data formatting | bytes 5242880 | tf_op jit(solution)/shard_map/reshape | solution.py:198
  202.0 2.7 fusion.6
  204.8 0.8 fusion.2
  205.7 0.8 fusion.1
  206.6 0.7 copy.128
  207.3 67.2 %all_to_all.42 = bf16[16,32,20,128]{3,1,2,0:T(8,128)(2,1)} all-to-all(bf16[16,32,20,128]{3,1,2,0:T(8,128)(2,1)S(1)} %bitcast.151), channel_id=1, replica_groups=mesh['sp'=32,'tp'=16] {'tp'}, dimensions={0} | all-to-all | bytes 5242880 | tf_op jit(solution)/shard_map/all_to_all | solution.py:76
  274.5 2.1 reduce_sum.85
  276.6 0.7 copy.106
  277.4 5.0 %all-to-all-start.5 = ((bf16[32,20,128]{2,1,0:T(8,128)(2,1)}), bf16[32,20,128]{2,1,0:T(8,128)(2,1)S(1)}, u32[]{:S(2)}, u32[]{:S(2)}) async-start(bf16[32,20,128]{2,1,0:T(8,128)(2,1)} %copy.106), calls=%async_computation.5 | async-start | bytes 393216 | tf_op jit(solution)/shard_map/all_to_all | solution.py:205
  282.3 0.1 reshape.391
  282.5 0.1 copy.98
  282.6 11.3 %all-to-all-done.5 = bf16[32,20,128]{2,1,0:T(8,128)(2,1)S(1)} async-done(((bf16[32,20,128]{2,1,0:T(8,128)(2,1)}), bf16[32,20,128]{2,1,0:T(8,128)(2,1)S(1)}, u32[]{:S(2)}, u32[]{:S(2)}) %all-to-all-start.5) | async-done | bytes 163872 | tf_op jit(solution)/shard_map/all_to_all | solution.py:205
  294.0 1.3 gather_fusion.1
  295.4 0.4 fusion.9
  295.8 11.1 %all_to_all.43 = bf16[16,16,128]{2,1,0:T(8,128)(2,1)S(1)} all-to-all(bf16[16,16,128]{2,1,0:T(8,128)(2,1)S(1)} %bitcast.166), channel_id=1, replica_groups=mesh['sp'=32,'tp'=16] {'tp'}, dimensions={0} | all-to-all | bytes 131072 | tf_op jit(solution)/shard_map/all_to_all | solution.py:210
  306.9 0.1 fusion.14
  307.0 0.7 fusion.18
  (93 shorter events, 1.7 us)
Async XLA Ops:
  0.0 205.7 %copy-start = (bf16[1,256,2048]{2,1,0:T(8,128)(2,1)S(1)}, bf16[1,256,2048]{2,1,0:T(8,128)(2,1)}, u32[]{:S(2)}) copy-start(bf16[1,256,2048]{2,1,0:T(8,128)(2,1)} %param.35) | copy-start | bytes 3145732
  0.0 19.8 %copy-start.4 = (bf16[256,64]{0,1:T(8,128)(2,1)S(1)}, bf16[256,64]{0,1:T(8,128)(2,1)}, u32[]{:S(2)}) copy-start(bf16[256,64]{0,1:T(8,128)(2,1)} %param.21) | copy-start | bytes 98308
  0.0 20.3 %copy-start.2 = (bf16[256,128]{1,0:T(8,128)(2,1)S(1)}, bf16[256,128]{1,0:T(8,128)(2,1)}, u32[]{:S(2)}) copy-start(bf16[256,128]{1,0:T(8,128)(2,1)} %param.22) | copy-start | bytes 196612
  0.0 20.0 %copy-start.7 = (bf16[256,64]{0,1:T(8,128)(2,1)S(1)}, bf16[256,64]{0,1:T(8,128)(2,1)}, u32[]{:S(2)}) copy-start(bf16[256,64]{0,1:T(8,128)(2,1)} %param.20) | copy-start | bytes 98308
  6.0 31.3 %all-to-all-start = ((bf16[32,65,128]{2,1,0:T(8,128)(2,1)}), bf16[32,65,128]{2,1,0:T(8,128)(2,1)S(1)}, u32[]{:S(2)}, u32[]{:S(2)}) async-start(bf16[32,65,128]{2,1,0:T(8,128)(2,1)} %broadcast_in_dim.52), calls=%async_computation | async-start | bytes 1179648 | tf_op jit(solution)/shard_map/all_to_all | solution.py:19
  37.8 1.7 copy-start.5
  37.8 1.7 copy-start.13
  37.8 1.8 copy-start.3
  39.5 38.6 %copy-start.6 = (bf16[16,2048]{1,0:T(8,128)(2,1)S(1)}, bf16[16,2048]{1,0:T(8,128)(2,1)}, u32[]{:S(2)}) copy-start(bf16[16,2048]{1,0:T(8,128)(2,1)} %param.29) | copy-start | bytes 196612
  39.5 38.6 %copy-start.8 = (f32[2048]{0:T(1024)S(1)}, f32[2048]{0:T(1024)}, u32[]{:S(2)}) copy-start(f32[2048]{0:T(1024)} %param.30) | copy-start | bytes 24580
  39.6 38.7 %copy-start.9 = (f32[2048]{0:T(1024)S(1)}, f32[2048]{0:T(1024)}, u32[]{:S(2)}) copy-start(f32[2048]{0:T(1024)} %param.31) | copy-start | bytes 24580
  77.8 5.3 %copy-start.11 = (s32[256,2]{0,1:T(2,128)S(1)}, s32[256,2]{0,1:T(2,128)}, u32[]{:S(2)}) copy-start(s32[256,2]{0,1:T(2,128)} %param.36) | copy-start | bytes 6148
  79.5 30.9 %all-to-all-start.2 = ((bf16[16,16,2048]{2,1,0:T(8,128)(2,1)}), bf16[16,16,2048]{2,1,0:T(8,128)(2,1)S(1)}, u32[]{:S(2)}, u32[]{:S(2)}) async-start(bf16[16,16,2048]{2,1,0:T(8,128)(2,1)} %broadcast_in_dim.57), calls=%async_computation.2 | async-start | bytes 2097152 | tf_op jit(solution)/shard_map/all_to_all | solution.py:19
  196.7 5.3 %copy-start.14 = (bf16[1,2048,256]{2,1,0:T(8,128)(2,1)S(1)}, bf16[1,2048,256]{2,1,0:T(8,128)(2,1)}, u32[]{:S(2)}) copy-start(bf16[1,2048,256]{2,1,0:T(8,128)(2,1)} %param.33) | copy-start | bytes 3145732
  202.0 2.8 copy-start.1
  202.0 2.8 copy-start.15
  274.5 8.0 %copy-start.12 = (f32[256,2]{0,1:T(2,128)S(1)}, f32[256,2]{0,1:T(2,128)}, u32[]{:S(2)}) copy-start(f32[256,2]{0,1:T(2,128)} %param.37) | copy-start | bytes 6148
  274.5 32.5 %copy-start.10 = (f32[2048]{0:T(1024)S(1)}, f32[2048]{0:T(1024)}, u32[]{:S(2)}) copy-start(f32[2048]{0:T(1024)} %param.32) | copy-start | bytes 24580
  277.4 16.6 %all-to-all-start.5 = ((bf16[32,20,128]{2,1,0:T(8,128)(2,1)}), bf16[32,20,128]{2,1,0:T(8,128)(2,1)S(1)}, u32[]{:S(2)}, u32[]{:S(2)}) async-start(bf16[32,20,128]{2,1,0:T(8,128)(2,1)} %copy.106), calls=%async_computation.5 | async-start | bytes 393216 | tf_op jit(solution)/shard_map/all_to_all | solution.py:205
where the time goes:
time: 309 us; the launch traced here: 308 us
  blocking collectives  193 us (62%)
  waiting for transfers between devices  50 us (16%)
  local copies, waits for them, and re-layouts  25.3 us (8%)
  starting transfers between devices  22.2 us (7%)
  other arithmetic  9.47 us (3%)
  matrix products  7.06 us (2%)
    all_to_all x2, blocking collectives, sum_at_owner(): parts = lax.all_to_all(split_up(shard, dim, peers), axis, 0, 0, tiled=True)  105 us
    all_to_all x1, blocking collectives, shards(): lax.all_to_all(outgoing, 'sp', split_axis=0, concat_axis=0, tiled=True)  77 us
    all_to_all x2, waiting for transfers between devices, copy_for_each(): lax.all_to_all(jnp.broadcast_to(shard[None], (peers, *shard.shape)), axis...  38.7 us
    all_to_all x2, starting transfers between devices, copy_for_each(): lax.all_to_all(jnp.broadcast_to(shard[None], (peers, *shard.shape)), axis...  17.3 us
    all_to_all x1, waiting for transfers between devices, shards(): lax.all_to_all(share_part, 'sp', split_axis=0, concat_axis=0, tiled=True)  11.3 us
    all_to_all x1, blocking collectives, shards(): lax.all_to_all(column_sums.astype(jnp.bfloat16), 'tp', split_axis=0, conc...  11.1 us
    gather x2, local copies, waits for them, and re-layouts, shards(): outgoing = block_rows[owners]  9.26 us
  transfers between devices with their start and end apart: 3, of which 3 were waited for; matrix products, arithmetic and copies ran while one was open for 2% of the time, Pallas kernels for 0%

commit v1 on v0

--- a/solution.py
+++ b/solution.py
@@ -1,17 +1,508 @@
+import functools
+
 import jax
 import jax.numpy as jnp
+import numpy as np
 from jax import lax
+from jax.experimental import pallas as pl
+from jax.experimental.pallas import tpu as pltpu
 from jax.sharding import PartitionSpec as P
 
 KEY_CHANNELS = 64
 DV = 128
 TOP = 2
 BLOCK = 64
-
+GROUP_SIZE = 4
+CORES = 2
 
 EPSILON = 1e-06
 DECAY_NORMALIZER = 16.0
 HIGHEST = lax.Precision.HIGHEST
+MESH = pl.DeviceIdType.MESH
+BF16 = jnp.bfloat16
+F32 = jnp.float32
+
+
+def dot(a, b):
+    return jnp.dot(a, b, preferred_element_type=F32)
+
+
+class Place:
+    def __init__(self, n_sp, n_tp, group):
+        self.X, self.Z = group, n_sp // group
+        self.C, self.Y = CORES, n_tp // CORES
+        self.n_tp = n_tp
+        self.sp, self.tp = lax.axis_index("sp"), lax.axis_index("tp")
+        self.z, self.x = self.sp // self.X, self.sp % self.X
+        self.y, self.c = self.tp // self.C, self.tp % self.C
+
+    def at(self, z=None, x=None, y=None, c=None):
+        z = self.z if z is None else z
+        x = self.x if x is None else x
+        y = self.y if y is None else y
+        c = self.c if c is None else c
+        return (z * self.X + x, y * self.C + c)
+
+
+def remote(src, dst, send, recv, to):
+    return pltpu.make_async_remote_copy(
+        src_ref=src, dst_ref=dst, send_sem=send, recv_sem=recv, device_id=to, device_id_type=MESH
+    )
+
+
+def ring_index(way, step, half, steps):
+    return way * (2 * steps - 1) + (0 if step == 1 else 1 + (step - 2) * 2 + half)
+
+
+def ring_sum(at, part, out, sends, recvs, send_sems, recv_sems):
+    Y, steps, y = at.Y, at.Y // 2, at.y
+
+    def copy(way, step, half):
+        i = ring_index(way, step, half, steps)
+        to = (y + 1) % Y if way == 0 else (y + Y - 1) % Y
+        return remote(sends.at[i], recvs.at[i], send_sems.at[i], recv_sems.at[i], at.at(y=to))
+
+    def offset(way, step):
+        k = steps - step + 1
+        return k if way == 0 or k == steps else -k
+
+    started = []
+
+    def send(way, step, half, value):
+        sends[ring_index(way, step, half, steps)] = value.astype(BF16)
+        c = copy(way, step, half)
+        c.start()
+        started.append(c)
+
+    for way, half in ((0, 0), (1, 1)):
+        send(way, 1, half, part(offset(way, 1), half))
+    for step in range(2, steps + 1):
+        for way, half in ((0, 1), (1, 0), (0, 0), (1, 1)):
+            value = part(offset(way, step), half)
+            if step > 2 or way == half:
+                copy(way, step - 1, half).wait_recv()
+                value = value + recvs[ring_index(way, step - 1, half, steps)].astype(F32)
+            send(way, step, half, value)
+    for half in (0, 1):
+        total = part(0, half)
+        for way in (0, 1):
+            copy(way, steps, half).wait_recv()
+            total = total + recvs[ring_index(way, steps, half, steps)].astype(F32)
+        out(half, total)
+    return started
+
+
+def layer_kernel(
+    n_sp, n_tp, group, cap,
+    gated, w_out, residual, attention_gain, before_gain, after_gain,
+    w_gate, w_up, w_down, ids_col, ids_row, weights, perm_out, perm_back,
+    out,
+    gu, wd, wo, partner, mixed, mid, normed, block, rows, acc, hid, shares, result,
+    zs, zr, xs, xb, zs2, zr2, column, branch,
+    sa, ra, sb, rb,
+    wsem, wrs, wrr, gsem, as_, ar, zss, zrs, xss, xrs, gs, gr, bs, br, xbs, xbr, zbs, zbr, fs,
+):
+    at = Place(n_sp, n_tp, group)
+    X, Y, Z, C = at.X, at.Y, at.Z, at.C
+    x, y, z, c = at.x, at.y, at.z, at.c
+    steps = Y // 2
+    other = 1 - c
+
+    local = [
+        pltpu.make_async_copy(w_gate, gu.at[0], wsem.at[0]),
+        pltpu.make_async_copy(w_up, gu.at[1], wsem.at[1]),
+        pltpu.make_async_copy(w_down, wd.at[0], wsem.at[2]),
+        pltpu.make_async_copy(w_out, wo.at[0], wsem.at[3]),
+    ]
+    local[3].start()
+    for k in (0, 1, 2):
+        local[k].start()
+
+    barrier = pltpu.get_barrier_semaphore()
+
+    def greet_tp(k, carry):
+        pl.semaphore_signal(barrier, inc=1, device_id=(at.sp, (at.tp + k) % n_tp), device_id_type=MESH)
+        return carry
+
+    lax.fori_loop(1, n_tp, greet_tp, 0)
+    for k in range(1, Z):
+        pl.semaphore_signal(barrier, inc=1, device_id=at.at(z=(z + k) % Z), device_id_type=MESH)
+    for k in range(1, X):
+        for core in range(C):
+            pl.semaphore_signal(barrier, inc=1, device_id=at.at(x=(x + k) % X, c=core), device_id_type=MESH)
+    pl.semaphore_wait(barrier, n_tp - 1 + Z - 1 + (X - 1) * C)
+
+    pair = at.at(c=other)
+    swap = remote(gated.at[:, other], partner, gsem.at[0], gsem.at[1], pair)
+    swap.start()
+    crossed = [
+        remote(w_out, wo.at[1], wrs.at[3], wrr.at[3], pair),
+        remote(w_gate, gu.at[2], wrs.at[0], wrr.at[0], pair),
+        remote(w_up, gu.at[3], wrs.at[1], wrr.at[1], pair),
+        remote(w_down, wd.at[1], wrs.at[2], wrr.at[2], pair),
+    ]
+    for k in crossed:
+        k.start()
+
+    share = gated.shape[0]
+    piece = gated.shape[2]
+    width = wo.shape[2]
+    swap.wait_recv()
+    local[3].wait()
+    crossed[0].wait_recv()
+    mine = gated[:, pl.ds(c, 1)].reshape(share * piece, DV)
+    theirs = partner[...].reshape(share * piece, DV)
+    tile = width // 4
+    for k in range(4):
+        cols = slice(k * tile, (k + 1) * tile)
+        value = dot(mine, wo[0, :, cols]) + dot(theirs, wo[1, :, cols])
+        mixed[:, :, cols] = value.reshape(share, piece, tile)
+
+    half_width = width // 2
+
+    def mixed_part(k, half):
+        d = (y + k + Y) % Y
+        return mixed[pl.ds(d, 1), :, half * half_width : (half + 1) * half_width].reshape(piece, half_width)
+
+    total = [None, None]
+
+    def keep(half, value):
+        total[half] = value
+
+    sum_a = ring_sum(at, mixed_part, keep, sa, ra, as_.at[0], as_.at[1])
+    attn = jnp.concatenate(total, axis=1)
+    attn = attn * lax.rsqrt(jnp.mean(attn * attn, axis=1, keepdims=True) + EPSILON) * attention_gain[...]
+    mid[...] = (residual[...].astype(F32) + attn).astype(BF16)
+    m = mid[...].astype(F32)
+    m = m * lax.rsqrt(jnp.mean(m * m, axis=1, keepdims=True) + EPSILON) * before_gain[...]
+    normed[...] = m.astype(BF16)
+
+    def share_cols(t):
+        return pl.ds(pl.multiple_of(t * DV, DV), DV)
+
+    def share_rows(t):
+        return pl.ds(pl.multiple_of(t * piece, piece), piece)
+
+    def to_width(k):
+        t = (at.tp + k) % n_tp
+        return remote(
+            normed.at[:, share_cols(t)], block.at[share_rows(at.tp), :], ar.at[0, k], ar.at[1, k], (at.sp, t)
+        )
+
+    def start_width(k, carry):
+        to_width(k).start()
+        return carry
+
+    def wait_width(k, carry):
+        to_width(k).wait_recv()
+        return carry
+
+    lax.fori_loop(1, n_tp, start_width, 0)
+    block[share_rows(at.tp), :] = normed[:, share_cols(at.tp)]
+
+    tokens = block.shape[0]
+    slots = n_sp * cap
+    lane = lax.broadcasted_iota(jnp.int32, (tokens, n_sp), 1)
+    e0, e1 = ids_col[:, 0:1], ids_col[:, 1:2]
+    r, q = (lax.broadcasted_iota(jnp.int32, (tokens, tokens), k) for k in (0, 1))
+    named = jnp.where((lane == e0) | (lane == e1), 1.0, 0.0).astype(BF16)
+    before = dot(jnp.where(r > q, 1.0, 0.0).astype(BF16), named)
+    wide = lax.broadcasted_iota(jnp.int32, (tokens, slots), 1)
+    picks = []
+    for e in (e0, e1):
+        slot = jnp.sum(jnp.where(lane == e, before, 0.0), axis=1, keepdims=True)
+        picks.append(e * cap + slot.astype(jnp.int32))
+    sub = lax.broadcasted_iota(jnp.int32, (n_sp, tokens), 0)
+    f0, f1 = ids_row[0:1, :], ids_row[1:2, :]
+    named_t = jnp.where((sub == f0) | (sub == f1), 1.0, 0.0).astype(BF16)
+    before_t = dot(named_t, jnp.where(r < q, 1.0, 0.0).astype(BF16))
+    tall = lax.broadcasted_iota(jnp.int32, (slots, tokens), 0)
+    spread = None
+    for f in (f0, f1):
+        slot = jnp.sum(jnp.where(sub == f, before_t, 0.0), axis=0, keepdims=True)
+        hit = jnp.where(tall == f * cap + slot.astype(jnp.int32), 1.0, 0.0)
+        spread = hit if spread is None else spread + hit
+    spread = spread.astype(BF16)
+
+    lax.fori_loop(1, n_tp, wait_width, 0)
+    picked = dot(spread, block[...]).astype(BF16)
+    zs[...] = picked.reshape(zs.shape)
+
+    def z_out(k):
+        return remote(zs.at[(z + k) % Z], zr.at[z], zss.at[k], zrs.at[k], at.at(z=(z + k) % Z))
+
+    for k in range(1, Z):
+        z_out(k).start()
+    zr[pl.ds(z, 1)] = zs[pl.ds(z, 1)]
+    for k in range(1, Z):
+        z_out(k).wait_recv()
+
+    order = lax.broadcasted_iota(jnp.int32, (slots, slots), 1)
+    turn = jnp.where(order == perm_out[...], 1.0, 0.0).astype(BF16)
+    xs[...] = dot(turn, zr[...].reshape(slots, DV)).astype(BF16).reshape(xs.shape)
+
+    side = x % C
+    mine_half = x // C
+
+    def x_out(k):
+        to = (x + k) % X
+        return (
+            xs.at[to],
+            rows.at[y, mine_half, :, share_cols(c)],
+            xss.at[k],
+            xrs.at[mine_half, c],
+            at.at(x=to, c=side),
+        )
+
+    for k in range(1, X):
+        remote(*x_out(k)).start()
+    src, dst, s_sem, r_sem, to = x_out(0)
+
+    @pl.when(side == c)
+    def _():
+        pltpu.make_async_copy(src, dst, r_sem).start()
+
+    @pl.when(side != c)
+    def _():
+        remote(src, dst, s_sem, r_sem, pair).start()
+
+    def gather(way, step, half):
+        j = (y + Y - (step - 1)) % Y if way == 0 else (y + step - 1) % Y
+        to = (y + 1) % Y if way == 0 else (y + Y - 1) % Y
+        i = way * (2 * steps - 1) + (step - 1) * 2 + (half if step < steps else 0)
+        return remote(rows.at[j, half], rows.at[j, half], gs.at[i], gr.at[i], at.at(y=to))
+
+    gathers = []
+
+    def start_gather(way, step, half):
+        g = gather(way, step, half)
+        g.start()
+        gathers.append(g)
+
+    for half in (0, 1):
+        for core in range(C):
+            pltpu.make_async_copy(xs.at[0], rows.at[y, half, :, pl.ds(core * DV, DV)], xrs.at[half, core]).wait()
+        for way in (0, 1):
+            start_gather(way, 1, half)
+
+    count = rows.shape[1] * rows.shape[2]
+    chunk = rows.shape[3]
+    local[0].wait()
+    local[1].wait()
+    crossed[1].wait_recv()
+    crossed[2].wait_recv()
+
+    def grow(j, first=False):
+        a = rows[pl.ds(j, 1)].reshape(count, chunk)
+        at_rows = pl.ds(pl.multiple_of(j * chunk, chunk), chunk)
+        for k in range(4):
+            value = dot(a, gu[k, at_rows, :])
+            acc[k] = value if first else acc[k] + value
+
+    grow(y, True)
+    for step in range(1, steps):
+        for half in (0, 1):
+            for way in (0, 1):
+                gather(way, step, half).wait_recv()
+                if step + 1 < steps or way == half:
+                    start_gather(way, step + 1, half)
+        grow((y + Y - step) % Y)
+        grow((y + step) % Y)
+    for way in (0, 1):
+        gather(way, steps, way).wait_recv()
+    grow((y + steps) % Y)
+
+    for k in (0, 1):
+        gate, up = acc[2 * k], acc[2 * k + 1]
+        hid[k] = (gate * jax.nn.sigmoid(gate) * up).astype(BF16)
+
+    local[2].wait()
+    crossed[3].wait_recv()
+    made = {}
+
+    def down(offset):
+        d = (y + offset + Y) % Y
+        cols = pl.ds(pl.multiple_of(d * chunk, chunk), chunk)
+        value = dot(hid[0], wd[0, :, cols]) + dot(hid[1], wd[1, :, cols])
+        shares[offset + steps - 1] = value.reshape(2, count // 2, chunk)
+
+    def down_part(offset, half):
+        if offset not in made:
+            down(offset)
+            made[offset] = True
+        return shares[offset + steps - 1, half]
+
+    def keep_result(half, value):
+        result[half] = value.astype(BF16)
+
+    sum_b = ring_sum(at, down_part, keep_result, sb, rb, bs, br)
+
+    def x_back(half, core):
+        home = 2 * half + c
+        return (
+            result.at[half, :, pl.ds(core * DV, DV)],
+            xb.at[x],
+            xbs.at[2 * half + core],
+            xbr.at[x],
+            at.at(x=home, c=core),
+        ), (home == x) & (c == core)
+
+    for half in (0, 1):
+        for core in range(C):
+            args, here = x_back(half, core)
+
+            @pl.when(here)
+            def _(args=args):
+                pltpu.make_async_copy(args[0], args[1], args[3]).start()
+
+            @pl.when(jnp.logical_not(here))
+            def _(args=args):
+                remote(*args).start()
+
+    for k in range(X):
+        pltpu.make_async_copy(xs.at[0], xb.at[k], xbr.at[k]).wait()
+    turn = jnp.where(order == perm_back[...], 1.0, 0.0).astype(BF16)
+    zs2[...] = dot(turn, xb[...].reshape(slots, DV)).astype(BF16).reshape(zs2.shape)
+
+    def z_back(k):
+        return remote(zs2.at[(z + k) % Z], zr2.at[z], zbs.at[k], zbr.at[k], at.at(z=(z + k) % Z))
+
+    for k in range(1, Z):
+        z_back(k).start()
+    zr2[pl.ds(z, 1)] = zs2[pl.ds(z, 1)]
+    finds = [jnp.where(wide == p, 1.0, 0.0).astype(BF16) for p in picks]
+    for k in range(1, Z):
+        z_back(k).wait_recv()
+    lookup = zr2[...].reshape(slots, DV)
+    column[...] = (
+        weights[:, 0:1] * dot(finds[0], lookup) + weights[:, 1:2] * dot(finds[1], lookup)
+    ).astype(BF16)
+
+    def to_rows(k):
+        t = (at.tp + k) % n_tp
+        return remote(
+            column.at[share_rows(t), :], branch.at[:, share_cols(at.tp)], fs.at[0, k], fs.at[1, k], (at.sp, t)
+        )
+
+    def start_rows(k, carry):
+        to_rows(k).start()
+        return carry
+
+    def wait_rows(k, carry):
+        to_rows(k).wait_recv()
+        return carry
+
+    lax.fori_loop(1, n_tp, start_rows, 0)
+    branch[:, share_cols(at.tp)] = column[share_rows(at.tp), :]
+    lax.fori_loop(1, n_tp, wait_rows, 0)
+    b = branch[...].astype(F32)
+    b = b * lax.rsqrt(jnp.mean(b * b, axis=1, keepdims=True) + EPSILON) * after_gain[...]
+    out[...] = (mid[...].astype(F32) + b).astype(BF16)
+
+    swap.wait_send()
+    for k in crossed + sum_a + gathers + sum_b:
+        k.wait_send()
+
+    def wait_sent(k, carry):
+        to_width(k).wait_send()
+        to_rows(k).wait_send()
+        return carry
+
+    lax.fori_loop(1, n_tp, wait_sent, 0)
+    for k in range(1, Z):
+        z_out(k).wait_send()
+        z_back(k).wait_send()
+    for k in range(1, X):
+        remote(*x_out(k)).wait_send()
+
+    @pl.when(side != c)
+    def _():
+        remote(src, dst, s_sem, r_sem, pair).wait_send()
+
+    for half in (0, 1):
+        for core in range(C):
+            args, here = x_back(half, core)
+
+            @pl.when(jnp.logical_not(here))
+            def _(args=args):
+                remote(*args).wait_send()
+
+
+def layer_tail(
+    gated, output_projection, residual, attention_gain, before_gain, after_gain,
+    w_gate, w_up, w_down, ids, weights,
+):
+    n_sp, n_tp = lax.axis_size("sp"), lax.axis_size("tp")
+    tokens, width = gated.shape[0], residual.shape[1]
+    piece = residual.shape[0]
+    X, C = GROUP_SIZE, CORES
+    Z, Y = n_sp // X, n_tp // C
+    cap = 5 * tokens // (2 * n_sp)
+    slots = n_sp * cap
+    steps = Y // 2
+    msgs = 2 * (2 * steps - 1)
+    half = slots // 4
+    chunk = C * DV
+    hidden = w_gate.shape[2]
+    order = np.arange(slots).reshape(Z, X, cap)
+    perm_out = np.transpose(order, (1, 0, 2)).reshape(slots, 1).astype(np.int32)
+    order = np.arange(slots).reshape(X, Z, cap)
+    perm_back = np.transpose(order, (1, 0, 2)).reshape(slots, 1).astype(np.int32)
+    vm, hbm = pl.BlockSpec(memory_space=pltpu.VMEM), pl.BlockSpec(memory_space=pl.ANY)
+    sem = pltpu.SemaphoreType.DMA
+    scratch = [
+        pltpu.VMEM((4, width, hidden), BF16),
+        pltpu.VMEM((2, hidden, width), BF16),
+        pltpu.VMEM((2, DV, width), BF16),
+        pltpu.VMEM((Y, piece, DV), BF16),
+        pltpu.VMEM((Y, piece, width), F32),
+        pltpu.VMEM((piece, width), BF16),
+        pltpu.VMEM((piece, width), BF16),
+        pltpu.VMEM((tokens, DV), BF16),
+        pltpu.VMEM((Y, 2, half, chunk), BF16),
+        pltpu.VMEM((4, 2 * half, hidden), F32),
+        pltpu.VMEM((2, 2 * half, hidden), BF16),
+        pltpu.VMEM((Y, 2, half, chunk), F32),
+        pltpu.VMEM((2, half, chunk), BF16),
+        pltpu.VMEM((Z, X * cap, DV), BF16),
+        pltpu.VMEM((Z, X * cap, DV), BF16),
+        pltpu.VMEM((X, Z * cap, DV), BF16),
+        pltpu.VMEM((X, Z * cap, DV), BF16),
+        pltpu.VMEM((Z, X * cap, DV), BF16),
+        pltpu.VMEM((Z, X * cap, DV), BF16),
+        pltpu.VMEM((tokens, DV), BF16),
+        pltpu.VMEM((piece, width), BF16),
+        pltpu.VMEM((msgs, piece, width // 2), BF16),
+        pltpu.VMEM((msgs, piece, width // 2), BF16),
+        pltpu.VMEM((msgs, half, chunk), BF16),
+        pltpu.VMEM((msgs, half, chunk), BF16),
+        sem((4,)), sem((4,)), sem((4,)), sem((2,)),
+        sem((2, msgs)),
+        sem((2, n_tp)),
+        sem((Z,)), sem((Z,)),
+        sem((X,)), sem((2, C)),
+        sem((msgs,)), sem((msgs,)),
+        sem((msgs,)), sem((msgs,)),
+        sem((2 * C,)), sem((X,)),
+        sem((Z,)), sem((Z,)),
+        sem((2, n_tp)),
+    ]
+    return pl.pallas_call(
+        functools.partial(layer_kernel, n_sp, n_tp, X, cap),
+        out_shape=jax.ShapeDtypeStruct((piece, width), BF16),
+        in_specs=[vm, hbm, vm, vm, vm, vm, hbm, hbm, hbm, vm, vm, vm, vm, vm],
+        out_specs=vm,
+        scratch_shapes=scratch,
+        name="layer_tail",
+        compiler_params=pltpu.CompilerParams(
+            collective_id=0, has_side_effects=True, vmem_limit_bytes=60 * 1024 * 1024
+        ),
+    )(
+        gated.reshape(Y, C, piece, DV), output_projection, residual,
+        attention_gain[None], before_gain[None], after_gain[None],
+        w_gate[0], w_up[0], w_down[0], ids, ids.T, weights,
+        jnp.asarray(perm_out), jnp.asarray(perm_back),
+    )
 
 
 def copy_for_each(shard, axis):
@@ -63,28 +554,6 @@
         axis,
     )
     return combined_pairwise(jax.tree.map(kept, pieces, identity, shard), combine)
-
-
-def split_up(shard, dim, peers):
-    shape = shard.shape
-    parts = shard.reshape(*shape[:dim], peers, shape[dim] // peers, *shape[dim + 1 :])
-    return jnp.moveaxis(parts, dim, 0)
-
-
-def sum_at_owner(shard, axis, dim):
-    peers = lax.axis_size(axis)
-    parts = lax.all_to_all(split_up(shard, dim, peers), axis, 0, 0, tiled=True)
-    return jnp.sum(parts.astype(jnp.float32), axis=0)
-
-
-def laid_out(parts, dim):
-    parts = jnp.moveaxis(parts, 0, dim)
-    shape = parts.shape
-    return parts.reshape(*shape[:dim], shape[dim] * shape[dim + 1], *shape[dim + 2 :])
-
-
-def collect(shard, axis, dim):
-    return laid_out(copy_for_each(shard, axis), dim)
 
 
 def rms_scale(values, gain_row):
@@ -171,47 +640,9 @@
         .astype(jnp.bfloat16)
         .reshape(sequence_length, number_heads * DV)
     )
-    mixed = sum_at_owner(
-        jnp.dot(gated, output_projection, preferred_element_type=jnp.float32).astype(jnp.bfloat16),
-        "tp",
-        0,
-    )
-    layer_mid = (residual_input.astype(jnp.float32) + rms_scale(mixed, attention_norm_gain)).astype(
-        jnp.bfloat16
-    )
-    normed = rms_scale(layer_mid.astype(jnp.float32), expert_before_gain).astype(jnp.bfloat16)
-    block_rows = collect(normed, "tp", 0)
-    expert_count = lax.axis_size("sp")
-    capacity = 5 * sequence_length // (2 * expert_count)
-    flat_ids = token_expert_index.reshape(sequence_length * TOP)
-    one_hot = (flat_ids[:, None] == jnp.arange(expert_count, dtype=jnp.int32)[None, :]).astype(
-        jnp.int32
-    )
-    slot_index = jnp.sum((jnp.cumsum(one_hot, axis=0) - one_hot) * one_hot, axis=1)
-    target = flat_ids * capacity + slot_index
-    owners = jnp.zeros((expert_count * capacity,), jnp.int32)
-    owners = owners.at[target].set(jnp.arange(sequence_length * TOP, dtype=jnp.int32) // TOP)
-    owners = owners.reshape(expert_count, capacity)
-    outgoing = block_rows[owners]
-    arrived = lax.all_to_all(outgoing, "sp", split_axis=0, concat_axis=0, tiled=True)
-    sources, slot_count, col_count = arrived.shape
-    rows_in = arrived.reshape(sources * slot_count, col_count)
-    gate_part = jnp.dot(rows_in, expert_gate_weight[0], preferred_element_type=jnp.float32)
-    up_part = jnp.dot(rows_in, expert_up_weight[0], preferred_element_type=jnp.float32)
-    hidden = (jax.nn.silu(gate_part) * up_part).astype(jnp.bfloat16)
-    partial_value = jnp.dot(hidden, expert_down_weight[0], preferred_element_type=jnp.float32)
-    partial_value = partial_value.reshape(sources, slot_count, col_count)
-    share_part = sum_at_owner(partial_value.astype(jnp.bfloat16), "tp", 2).astype(jnp.bfloat16)
-    back_rows = lax.all_to_all(share_part, "sp", split_axis=0, concat_axis=0, tiled=True)
-    lookup = back_rows.reshape(expert_count * capacity, back_rows.shape[2])
-    token_target = target.reshape(sequence_length, TOP)
-    picked = lookup[token_target].astype(jnp.float32)
-    column_sums = jnp.sum(routing_weight_matrix[:, :, None] * picked, axis=1)
-    branch = lax.all_to_all(
-        column_sums.astype(jnp.bfloat16), "tp", split_axis=0, concat_axis=1, tiled=True
-    ).astype(column_sums.dtype)
-    return (layer_mid.astype(jnp.float32) + rms_scale(branch, expert_after_gain)).astype(
-        jnp.bfloat16
+    return layer_tail(
+        gated, output_projection, residual_input, attention_norm_gain, expert_before_gain, expert_after_gain,
+        expert_gate_weight, expert_up_weight, expert_down_weight, token_expert_index, routing_weight_matrix,
     )
 
 

time: 309 us -> 139 us (0.45)
  blocking collectives: 193 us -> 0 us
  Pallas kernels: 0 us -> 97.1 us
  waiting for transfers between devices: 50 us -> 13.6 us
  local copies, waits for them, and re-layouts: 25.3 us -> 8.56 us
  starting transfers between devices: 22.2 us -> 13.7 us
  matrix products: 7.06 us -> 1.37 us
  other arithmetic: 9.47 us -> 3.81 us
    all_to_all x4 -> x0, blocking collectives: 193 us -> none  [the longest x2 105 us: sum_at_owner(): parts = lax.all_to_all(split_up(shard, dim, peers), axis, 0, 0, tiled=True)]
    pallas_call x0 -> x1, Pallas kernels: none -> 97.1 us  [layer_tail(): pl.pallas_call(functools.partial(layer_kernel, n_sp, n_tp, X, cap), out_s...]
    all_to_all x2 -> x1, waiting for transfers between devices: 38.7 us -> 13.6 us  [copy_for_each(): lax.all_to_all(jnp.broadcast_to(shard[None], (peers, *shard.shape)), axis...]
    all_to_all x1 -> x0, waiting for transfers between devices: 11.3 us -> none  [shards(): lax.all_to_all(share_part, 'sp', split_axis=0, concat_axis=0, tiled=True)]
    gather x3 -> x0, local copies, waits for them, and re-layouts: 10.6 us -> none  [the longest x2 9.26 us: shards(): outgoing = block_rows[owners]]
    reshape x5 -> x1, local copies, waits for them, and re-layouts: 6.09 us -> 0.01 us  [the longest x1 5.28 us: shards(): rows_in = arrived.reshape(sources * slot_count, col_count)]
    unnamed x35 -> x22, local copies, waits for them, and re-layouts: 0.39 us -> 5.68 us
    all_to_all x1 -> x0, starting transfers between devices: 4.96 us -> none  [shards(): lax.all_to_all(share_part, 'sp', split_axis=0, concat_axis=0, tiled=True)]
  transfers between devices with their start and end apart: 3 -> 1, of which waited for: 3 -> 1; matrix products, arithmetic and copies ran while one was open for 2% -> 2% of each run, Pallas kernels for 0% -> 0%
where the time goes in v1:
time: 139 us; the launch traced here: 138 us
  Pallas kernels  97.1 us (70%)
  starting transfers between devices  13.7 us (10%)
  waiting for transfers between devices  13.6 us (10%)
  local copies, waits for them, and re-layouts  8.56 us (6%)
  other arithmetic  3.81 us (3%)
    pallas_call x1, Pallas kernels, layer_tail(): pl.pallas_call(functools.partial(layer_kernel, n_sp, n_tp, X, cap), out_s...  97.1 us
    all_to_all x1, starting transfers between devices, copy_for_each(): lax.all_to_all(jnp.broadcast_to(shard[None], (peers, *shard.shape)), axis...  13.7 us
    all_to_all x1, waiting for transfers between devices, copy_for_each(): lax.all_to_all(jnp.broadcast_to(shard[None], (peers, *shard.shape)), axis...  13.6 us
    unnamed x22, local copies, waits for them, and re-layouts  5.68 us
  transfers between devices with their start and end apart: 1, of which 1 were waited for; matrix products, arithmetic and copies ran while one was open for 2% of the time, Pallas kernels for 0%

profile of v1, /device:TPU:1, one launch (start us, length us, event | category | flops | bytes accessed | tf_op | source)
XLA Modules:
  0.0 138.5 jit_solution(15411765316568412965)
XLA Ops:
  0.0 0.0 copy-start
  0.0 0.0 copy-start.6
  0.0 0.0 copy-start.7
  0.0 0.7 copy-done.6
  0.7 0.0 copy-done.7
  0.7 0.9 fusion.19
  1.6 0.6 reduce-window.6
  2.2 0.2 slice_reduce_fusion
  2.4 0.1 copy.50
  2.5 0.1 copy.51
  2.6 0.1 broadcast.69
  2.7 0.1 add_bitcast_fusion
  2.8 0.0 copy-start.1
  2.8 0.9 slice_reduce_fusion.1
  3.8 0.0 copy-done.1
  3.8 0.2 exponential_multiply_fusion.3
  4.0 0.0 copy-done
  4.0 0.2 convolution_convert_fusion
  4.2 0.9 broadcast_in_dim.72
  5.1 13.7 %all-to-all-start = ((bf16[32,65,128]{2,1,0:T(8,128)(2,1)}), bf16[32,65,128]{2,1,0:T(8,128)(2,1)S(1)}, u32[]{:S(2)}, u32[]{:S(2)}) async-start(bf16[32,65,128]{2,1,0:T(8,128)(2,1)} %broadcast_in_dim.72), calls=%async_computation | async-start | bytes 1179648 | tf_op jit(solution)/shard_map/all_to_all | solution.py:510
  18.8 0.1 copy.48
  18.9 0.0 copy-start.3
  18.9 0.1 copy.59
  19.0 0.7 copy-done.3
  19.7 0.0 copy-start.4
  19.7 0.1 copy.46
  19.8 0.6 copy-done.4
  20.3 0.0 copy-start.5
  20.3 0.8 copy.56.ids_col
  21.1 0.0 copy-done.5
  21.1 0.8 copy.57.weights
  21.9 0.1 fusion.26
  22.1 0.3 convolution_bitcast_fusion
  22.4 0.4 convolution_select_fusion
  22.7 13.6 %all-to-all-done = bf16[32,65,128]{2,1,0:T(8,128)(2,1)S(1)} async-done(((bf16[32,65,128]{2,1,0:T(8,128)(2,1)}), bf16[32,65,128]{2,1,0:T(8,128)(2,1)S(1)}, u32[]{:S(2)}, u32[]{:S(2)}) %all-to-all-start) | async-done | bytes 532512 | tf_op jit(solution)/shard_map/all_to_all | solution.py:510
  36.4 0.1 select_bitcast_fusion.1
  36.6 0.1 select_bitcast_fusion
  36.8 0.2 slice_add_fusion
  37.0 0.1 slice_add_fusion.1
  37.1 0.1 slice_add_fusion.2
  37.2 0.1 slice_add_fusion.3
  37.3 0.1 fusion.23
  37.4 0.4 while.12
  37.4 0.1 bitcast_add_fusion.2
  37.5 0.1 bitcast_add_fusion.2
  37.6 0.1 bitcast_add_fusion.2
  37.7 0.1 bitcast_add_fusion.2
  37.8 0.3 fusion.8
  38.1 0.0 copy-start.2
  38.1 0.3 fusion.7
  38.4 0.1 rsqrt.12
  38.5 0.0 copy-start.8
  38.5 0.4 copy-done.2
  38.9 0.2 copy-done.8
  39.2 0.7 fusion.16
  39.9 97.1 %layer_tail.1 = bf16[16,2048]{1,0:T(8,128)(2,1)} custom-call(bf16[8,2,16,128]{3,2,1,0:T(8,128)(2,1)} %bitcast.111, bf16[128,2048]{1,0:T(8,128)(2,1)} %w_out.1, bf16[16,2048]{1,0:T(8,128)(2,1)} %residual.1, f32[1,2048]{1,0:T(1,128)} %bitcast.120, f32[1,2048]{1,0:T(1,128)} %bitcast.121, f32[1,2048]{1,0:T(1,128)} %bitcast.122, bf16[2048,256]{1,0:T(8,128)(2,1)} %bitcast.107, ...), custom_call_target="tpu_custom_call" | custom-call | tf_op jit(solution)/shard_map/layer_tail/pallas_call | solution.py:490
  137.0 1.5 %copy.84 = bf16[16,2048]{1,0:T(8,128)(2,1)} copy(bf16[16,2048]{1,0:T(8,128)(2,1)} %layer_tail.1) | data formatting | bytes 131072
  (36 shorter events, 0.4 us)
Async XLA Ops:
  0.0 4.0 %copy-start = (bf16[256,128]{1,0:T(8,128)(2,1)S(1)}, bf16[256,128]{1,0:T(8,128)(2,1)}, u32[]{:S(2)}) copy-start(bf16[256,128]{1,0:T(8,128)(2,1)} %param.24) | copy-start | bytes 196612
  0.0 0.7 copy-start.6
  0.0 0.7 copy-start.7
  2.8 0.9 copy-start.1
  5.1 31.3 %all-to-all-start = ((bf16[32,65,128]{2,1,0:T(8,128)(2,1)}), bf16[32,65,128]{2,1,0:T(8,128)(2,1)S(1)}, u32[]{:S(2)}, u32[]{:S(2)}) async-start(bf16[32,65,128]{2,1,0:T(8,128)(2,1)} %broadcast_in_dim.72), calls=%async_computation | async-start | bytes 1179648 | tf_op jit(solution)/shard_map/all_to_all | solution.py:510
  18.9 0.8 copy-start.3
  19.7 0.7 copy-start.4
  20.3 0.8 copy-start.5
  38.1 0.8 copy-start.2
  38.5 0.7 copy-start.8

commit v2 on v1

--- a/solution.py
+++ b/solution.py
@@ -1,8 +1,8 @@
+import contextlib
 import functools
 
 import jax
 import jax.numpy as jnp
-import numpy as np
 from jax import lax
 from jax.experimental import pallas as pl
 from jax.experimental.pallas import tpu as pltpu
@@ -17,10 +17,14 @@
 
 EPSILON = 1e-06
 DECAY_NORMALIZER = 16.0
-HIGHEST = lax.Precision.HIGHEST
 MESH = pl.DeviceIdType.MESH
 BF16 = jnp.bfloat16
 F32 = jnp.float32
+PROFILE = False
+
+
+def scope(name):
+    return jax.named_scope(name) if PROFILE else contextlib.nullcontext()
 
 
 def dot(a, b):
@@ -92,15 +96,37 @@
     return started
 
 
+def split(value):
+    high = value.astype(BF16)
+    rest = value - high.astype(F32)
+    middle = rest.astype(BF16)
+    return high, middle, (rest - middle.astype(F32)).astype(BF16)
+
+
+def standing(row, count):
+    square = (count, row.shape[1])
+    same = lax.broadcasted_iota(jnp.int32, square, 0) == lax.broadcasted_iota(jnp.int32, square, 1)
+    return jnp.sum(jnp.where(same, row, 0.0), axis=1, keepdims=True)
+
+
+def lying(col, width):
+    square = (col.shape[0], width)
+    same = lax.broadcasted_iota(jnp.int32, square, 0) == lax.broadcasted_iota(jnp.int32, square, 1)
+    return jnp.sum(jnp.where(same, col, 0.0), axis=0, keepdims=True)
+
+
 def layer_kernel(
     n_sp, n_tp, group, cap,
-    gated, w_out, residual, attention_gain, before_gain, after_gain,
-    w_gate, w_up, w_down, ids_col, ids_row, weights, perm_out, perm_back,
+    q_t, k_t, values, gate_rows, decay_t, bias, extra, head_gain,
+    w_out, residual, attention_gain, before_gain, after_gain,
+    w_gate, w_up, w_down, ids_row, weights_row,
     out,
+    gated, stack, spread, find, turn_out, turn_back, sx, rx, sz, rz,
     gu, wd, wo, partner, mixed, mid, normed, block, rows, acc, hid, shares, result,
     zs, zr, xs, xb, zs2, zr2, column, branch,
     sa, ra, sb, rb,
     wsem, wrs, wrr, gsem, as_, ar, zss, zrs, xss, xrs, gs, gr, bs, br, xbs, xbr, zbs, zbr, fs,
+    sxs, sxr, szs, szr,
 ):
     at = Place(n_sp, n_tp, group)
     X, Y, Z, C = at.X, at.Y, at.Z, at.C
@@ -118,6 +144,7 @@
     for k in (0, 1, 2):
         local[k].start()
 
+    rz[...] = jnp.zeros_like(rz)
     barrier = pltpu.get_barrier_semaphore()
 
     def greet_tp(k, carry):
@@ -130,11 +157,42 @@
     for k in range(1, X):
         for core in range(C):
             pl.semaphore_signal(barrier, inc=1, device_id=at.at(x=(x + k) % X, c=core), device_id_type=MESH)
+
+    tokens = q_t.shape[1]
+    blocks = tokens // BLOCK
+    pre = decay_t[...].astype(F32) + standing(bias[...], KEY_CHANNELS)
+    log_decay = -(jnp.maximum(-pre, 0.0) + jnp.log1p(jnp.exp(-jnp.abs(pre)))) / DECAY_NORMALIZER + extra[...]
+    r, q = (lax.broadcasted_iota(jnp.int32, (tokens, tokens), k) for k in (0, 1))
+    one_block = (r // BLOCK) == (q // BLOCK)
+    upto = jnp.where((r <= q) & one_block, 1.0, 0.0).astype(BF16)
+    inside = sum(dot(term, upto) for term in split(log_decay))
+    ends = [inside[:, (b + 1) * BLOCK - 1 : (b + 1) * BLOCK] for b in range(blocks)]
+    of_block = lax.broadcasted_iota(jnp.int32, (KEY_CHANNELS, tokens), 1) // BLOCK
+    keys = k_t[...].astype(F32)
+    to_end = [jnp.where(of_block == b, keys * jnp.exp(jnp.minimum(ends[b] - inside, 0.0)), 0.0) for b in range(blocks)]
+    vals = values[...]
+    growth = dot(jnp.concatenate(to_end, axis=0).astype(BF16), vals)
+    growth = [growth[b * KEY_CHANNELS : (b + 1) * KEY_CHANNELS] for b in range(blocks)]
+    fades = [jnp.exp(e) for e in ends]
+    state = growth[0]
+    for b in range(1, blocks):
+        state = fades[b] * state + growth[b]
+    fade_row = lying(jnp.exp(sum(ends)), DV)
+    tail = KEY_CHANNELS + 16
+
+    def message(ref, state_part, row):
+        ref[0:KEY_CHANNELS, :] = state_part.astype(BF16)
+        ref[KEY_CHANNELS:tail, :] = jnp.broadcast_to(row, (16, DV)).astype(BF16)
+
+    message(sx, state, fade_row)
     pl.semaphore_wait(barrier, n_tp - 1 + Z - 1 + (X - 1) * C)
 
+    def state_x(k):
+        return remote(sx, rx.at[x], sxs.at[k], sxr.at[k], at.at(x=(x + k) % X))
+
+    for k in range(1, X):
+        state_x(k).start()
     pair = at.at(c=other)
-    swap = remote(gated.at[:, other], partner, gsem.at[0], gsem.at[1], pair)
-    swap.start()
     crossed = [
         remote(w_out, wo.at[1], wrs.at[3], wrr.at[3], pair),
         remote(w_gate, gu.at[2], wrs.at[0], wrr.at[0], pair),
@@ -143,6 +201,93 @@
     ]
     for k in crossed:
         k.start()
+    rx[pl.ds(x, 1)] = sx[...].reshape(1, tail, DV)
+
+    slots = n_sp * cap
+    sub = lax.broadcasted_iota(jnp.int32, (n_sp, tokens), 0)
+    chosen = [ids_row[k : k + 1, :] for k in range(TOP)]
+    named = jnp.where((sub == chosen[0]) | (sub == chosen[1]), 1.0, 0.0).astype(BF16)
+    before = dot(named, jnp.where(r < q, 1.0, 0.0).astype(BF16))
+    targets = []
+    for e in chosen:
+        slot = jnp.sum(jnp.where(sub == e, before, 0.0), axis=0, keepdims=True)
+        targets.append(e * cap + slot.astype(jnp.int32))
+    query = q_t[...].astype(F32) * (KEY_CHANNELS**-0.5 * jnp.exp(inside))
+    stack[0:KEY_CHANNELS, :] = query
+    stack[KEY_CHANNELS:, :] = jnp.zeros((stack.shape[0] - KEY_CHANNELS, tokens), F32)
+    for k in range(TOP):
+        stack[KEY_CHANNELS + k : KEY_CHANNELS + k + 1, :] = targets[k].astype(F32)
+        stack[KEY_CHANNELS + TOP + k : KEY_CHANNELS + TOP + k + 1, :] = weights_row[k : k + 1, :]
+    stood = stack[...].T
+    query = stood[:, 0:KEY_CHANNELS].astype(BF16)
+    target_cols = [stood[:, KEY_CHANNELS + k : KEY_CHANNELS + k + 1].astype(jnp.int32) for k in range(TOP)]
+    weight_cols = [stood[:, KEY_CHANNELS + TOP + k : KEY_CHANNELS + TOP + k + 1] for k in range(TOP)]
+    scores = dot(query, (keys * jnp.exp(-inside)).astype(BF16))
+    scores = jnp.where((r >= q) & one_block, scores, 0.0).astype(BF16)
+    within = dot(scores, vals)
+
+    for k in range(1, X):
+        state_x(k).wait_recv()
+    plane, plane_row = rx[0, 0:KEY_CHANNELS].astype(F32), rx[0, KEY_CHANNELS:tail][0:1].astype(F32)
+    ahead, ahead_fade = jnp.zeros_like(state), jnp.ones((KEY_CHANNELS, 1), F32)
+    for k in range(X):
+        part, row = rx[k, 0:KEY_CHANNELS].astype(F32), rx[k, KEY_CHANNELS:tail][0:1].astype(F32)
+        fade = standing(row, KEY_CHANNELS)
+        ahead = jnp.where(k < x, fade * ahead + part, ahead)
+        ahead_fade = jnp.where(k < x, fade * ahead_fade, ahead_fade)
+        if k:
+            plane, plane_row = fade * plane + part, plane_row * row
+    message(sz, plane, plane_row)
+
+    def state_z(k):
+        return remote(sz, rz.at[z], szs.at[k], szr.at[k], at.at(z=(z + k) % Z))
+
+    for k in range(1, Z):
+
+        @pl.when(z + k < Z)
+        def _(k=k):
+            state_z(k).start()
+
+    tall = lax.broadcasted_iota(jnp.int32, (slots, tokens), 0)
+    hits = [jnp.where(tall == t, 1.0, 0.0) for t in targets]
+    spread[...] = (hits[0] + hits[1]).astype(BF16)
+    wide = lax.broadcasted_iota(jnp.int32, (tokens, slots), 1)
+    for k in range(TOP):
+        find[k] = jnp.where(wide == target_cols[k], 1.0, 0.0).astype(BF16)
+    lane = lax.broadcasted_iota(jnp.int32, (1, slots), 1)
+
+    def turned(outer, inner):
+        a = sum(jnp.where(lane >= k * inner * cap, 1, 0) for k in range(1, outer))
+        rest = lane - a * (inner * cap)
+        b = sum(jnp.where(rest >= k * cap, 1, 0) for k in range(1, inner))
+        return b * (outer * cap) + a * cap + (rest - b * cap)
+
+    down_rows = lax.broadcasted_iota(jnp.int32, (slots, slots), 0)
+    turn_out[...] = jnp.where(down_rows == turned(Z, X), 1.0, 0.0).astype(BF16)
+    turn_back[...] = jnp.where(down_rows == turned(X, Z), 1.0, 0.0).astype(BF16)
+    gate_act = gate_rows[...].astype(F32)
+    gate_act = gate_act * jax.nn.sigmoid(gate_act) * head_gain[...]
+
+    for k in range(1, Z):
+
+        @pl.when(z >= k)
+        def _(k=k):
+            state_z(k).wait_recv()
+
+    carried = jnp.zeros_like(state)
+    for k in range(Z - 1):
+        fade = standing(rz[k, KEY_CHANNELS:tail][0:1].astype(F32), KEY_CHANNELS)
+        carried = jnp.where(k < z, fade * carried + rz[k, 0:KEY_CHANNELS].astype(F32), carried)
+    running = ahead_fade * carried + ahead
+    across = []
+    for b in range(blocks):
+        across.append(dot(query[b * BLOCK : (b + 1) * BLOCK], running.astype(BF16)))
+        running = fades[b] * running + growth[b]
+    heads = within + jnp.concatenate(across, axis=0)
+    heads = heads * lax.rsqrt(jnp.mean(heads * heads, axis=1, keepdims=True) + EPSILON) * gate_act
+    gated[...] = heads.astype(BF16).reshape(gated.shape)
+    swap = remote(gated.at[:, other], partner, gsem.at[0], gsem.at[1], pair)
+    swap.start()
 
     share = gated.shape[0]
     piece = gated.shape[2]
@@ -200,32 +345,8 @@
     lax.fori_loop(1, n_tp, start_width, 0)
     block[share_rows(at.tp), :] = normed[:, share_cols(at.tp)]
 
-    tokens = block.shape[0]
-    slots = n_sp * cap
-    lane = lax.broadcasted_iota(jnp.int32, (tokens, n_sp), 1)
-    e0, e1 = ids_col[:, 0:1], ids_col[:, 1:2]
-    r, q = (lax.broadcasted_iota(jnp.int32, (tokens, tokens), k) for k in (0, 1))
-    named = jnp.where((lane == e0) | (lane == e1), 1.0, 0.0).astype(BF16)
-    before = dot(jnp.where(r > q, 1.0, 0.0).astype(BF16), named)
-    wide = lax.broadcasted_iota(jnp.int32, (tokens, slots), 1)
-    picks = []
-    for e in (e0, e1):
-        slot = jnp.sum(jnp.where(lane == e, before, 0.0), axis=1, keepdims=True)
-        picks.append(e * cap + slot.astype(jnp.int32))
-    sub = lax.broadcasted_iota(jnp.int32, (n_sp, tokens), 0)
-    f0, f1 = ids_row[0:1, :], ids_row[1:2, :]
-    named_t = jnp.where((sub == f0) | (sub == f1), 1.0, 0.0).astype(BF16)
-    before_t = dot(named_t, jnp.where(r < q, 1.0, 0.0).astype(BF16))
-    tall = lax.broadcasted_iota(jnp.int32, (slots, tokens), 0)
-    spread = None
-    for f in (f0, f1):
-        slot = jnp.sum(jnp.where(sub == f, before_t, 0.0), axis=0, keepdims=True)
-        hit = jnp.where(tall == f * cap + slot.astype(jnp.int32), 1.0, 0.0)
-        spread = hit if spread is None else spread + hit
-    spread = spread.astype(BF16)
-
     lax.fori_loop(1, n_tp, wait_width, 0)
-    picked = dot(spread, block[...]).astype(BF16)
+    picked = dot(spread[...], block[...]).astype(BF16)
     zs[...] = picked.reshape(zs.shape)
 
     def z_out(k):
@@ -237,9 +358,7 @@
     for k in range(1, Z):
         z_out(k).wait_recv()
 
-    order = lax.broadcasted_iota(jnp.int32, (slots, slots), 1)
-    turn = jnp.where(order == perm_out[...], 1.0, 0.0).astype(BF16)
-    xs[...] = dot(turn, zr[...].reshape(slots, DV)).astype(BF16).reshape(xs.shape)
+    xs[...] = dot(turn_out[...], zr[...].reshape(slots, DV)).astype(BF16).reshape(xs.shape)
 
     side = x % C
     mine_half = x // C
@@ -361,8 +480,7 @@
 
     for k in range(X):
         pltpu.make_async_copy(xs.at[0], xb.at[k], xbr.at[k]).wait()
-    turn = jnp.where(order == perm_back[...], 1.0, 0.0).astype(BF16)
-    zs2[...] = dot(turn, xb[...].reshape(slots, DV)).astype(BF16).reshape(zs2.shape)
+    zs2[...] = dot(turn_back[...], xb[...].reshape(slots, DV)).astype(BF16).reshape(zs2.shape)
 
     def z_back(k):
         return remote(zs2.at[(z + k) % Z], zr2.at[z], zbs.at[k], zbr.at[k], at.at(z=(z + k) % Z))
@@ -370,12 +488,11 @@
     for k in range(1, Z):
         z_back(k).start()
     zr2[pl.ds(z, 1)] = zs2[pl.ds(z, 1)]
-    finds = [jnp.where(wide == p, 1.0, 0.0).astype(BF16) for p in picks]
     for k in range(1, Z):
         z_back(k).wait_recv()
     lookup = zr2[...].reshape(slots, DV)
     column[...] = (
-        weights[:, 0:1] * dot(finds[0], lookup) + weights[:, 1:2] * dot(finds[1], lookup)
+        weight_cols[0] * dot(find[0], lookup) + weight_cols[1] * dot(find[1], lookup)
     ).astype(BF16)
 
     def to_rows(k):
@@ -399,6 +516,14 @@
     b = b * lax.rsqrt(jnp.mean(b * b, axis=1, keepdims=True) + EPSILON) * after_gain[...]
     out[...] = (mid[...].astype(F32) + b).astype(BF16)
 
+    for k in range(1, X):
+        state_x(k).wait_send()
+    for k in range(1, Z):
+
+        @pl.when(z + k < Z)
+        def _(k=k):
+            state_z(k).wait_send()
+
     swap.wait_send()
     for k in crossed + sum_a + gathers + sum_b:
         k.wait_send()
@@ -428,12 +553,12 @@
                 remote(*args).wait_send()
 
 
-def layer_tail(
-    gated, output_projection, residual, attention_gain, before_gain, after_gain,
-    w_gate, w_up, w_down, ids, weights,
+def shards(
+    query, key, value, gate_rows, decay, bias, extra, head_gain, output_projection, residual,
+    attention_gain, before_gain, after_gain, w_gate, w_up, w_down, ids, weights,
 ):
     n_sp, n_tp = lax.axis_size("sp"), lax.axis_size("tp")
-    tokens, width = gated.shape[0], residual.shape[1]
+    tokens, width = query.shape[0], residual.shape[1]
     piece = residual.shape[0]
     X, C = GROUP_SIZE, CORES
     Z, Y = n_sp // X, n_tp // C
@@ -444,13 +569,20 @@
     half = slots // 4
     chunk = C * DV
     hidden = w_gate.shape[2]
-    order = np.arange(slots).reshape(Z, X, cap)
-    perm_out = np.transpose(order, (1, 0, 2)).reshape(slots, 1).astype(np.int32)
-    order = np.arange(slots).reshape(X, Z, cap)
-    perm_back = np.transpose(order, (1, 0, 2)).reshape(slots, 1).astype(np.int32)
     vm, hbm = pl.BlockSpec(memory_space=pltpu.VMEM), pl.BlockSpec(memory_space=pl.ANY)
     sem = pltpu.SemaphoreType.DMA
+    message = (KEY_CHANNELS + 16, DV)
     scratch = [
+        pltpu.VMEM((Y, C, piece, DV), BF16),
+        pltpu.VMEM((128, tokens), F32),
+        pltpu.VMEM((slots, tokens), BF16),
+        pltpu.VMEM((TOP, tokens, slots), BF16),
+        pltpu.VMEM((slots, slots), BF16),
+        pltpu.VMEM((slots, slots), BF16),
+        pltpu.VMEM(message, BF16),
+        pltpu.VMEM((X, *message), BF16),
+        pltpu.VMEM(message, BF16),
+        pltpu.VMEM((Z, *message), BF16),
         pltpu.VMEM((4, width, hidden), BF16),
         pltpu.VMEM((2, hidden, width), BF16),
         pltpu.VMEM((2, DV, width), BF16),
@@ -486,163 +618,22 @@
         sem((2 * C,)), sem((X,)),
         sem((Z,)), sem((Z,)),
         sem((2, n_tp)),
+        sem((X,)), sem((X,)), sem((Z,)), sem((Z,)),
     ]
     return pl.pallas_call(
         functools.partial(layer_kernel, n_sp, n_tp, X, cap),
         out_shape=jax.ShapeDtypeStruct((piece, width), BF16),
-        in_specs=[vm, hbm, vm, vm, vm, vm, hbm, hbm, hbm, vm, vm, vm, vm, vm],
+        in_specs=[vm] * 8 + [hbm] + [vm] * 4 + [hbm] * 3 + [vm] * 2,
         out_specs=vm,
         scratch_shapes=scratch,
-        name="layer_tail",
+        name="layer",
         compiler_params=pltpu.CompilerParams(
             collective_id=0, has_side_effects=True, vmem_limit_bytes=60 * 1024 * 1024
         ),
     )(
-        gated.reshape(Y, C, piece, DV), output_projection, residual,
-        attention_gain[None], before_gain[None], after_gain[None],
-        w_gate[0], w_up[0], w_down[0], ids, ids.T, weights,
-        jnp.asarray(perm_out), jnp.asarray(perm_back),
-    )
-
-
-def copy_for_each(shard, axis):
-    peers = lax.axis_size(axis)
-    return lax.all_to_all(
-        jnp.broadcast_to(shard[None], (peers, *shard.shape)), axis, 0, 0, tiled=True
-    )
-
-
-def gathered_once(shard, axis):
-    leaves = jax.tree.leaves(shard)
-    turns = sorted(range(len(leaves)), key=lambda k: -leaves[k].size)
-    width = (1, *leaves[turns[0]].shape)[-1]
-    lines = [
-        jnp.pad(leaves[k].reshape(-1), (0, -leaves[k].size % width)).reshape(-1, width)
-        for k in turns
-    ]
-    both, at, found = (copy_for_each(jnp.concatenate(lines), axis), 0, {})
-    for k, line in zip(turns, lines):
-        section = both[:, at : at + len(line)].reshape(len(both), -1)
-        found[k] = section[:, : leaves[k].size].reshape(-1, *leaves[k].shape)
-        at += len(line)
-    numbers = iter(range(len(leaves)))
-    return jax.tree.map(lambda _: found[next(numbers)], shard)
-
-
-def combined_pairwise(pieces, combine):
-    while len(jax.tree.leaves(pieces)[0]) > 1:
-        pieces = jax.vmap(combine)(
-            *(jax.tree.map(lambda part: part[side::2], pieces) for side in (0, 1))
-        )
-    return jax.tree.map(lambda part: part[0], pieces)
-
-
-def carried_in(shard, axis, combine, identity):
-    peers, position = (lax.axis_size(axis), lax.axis_index(axis))
-    passed = jnp.arange(peers) < position
-
-    def kept(part, zero, own):
-        part = jnp.where(
-            passed.reshape(-1, *(1 for _ in own.shape)),
-            part.astype(own.dtype),
-            jnp.asarray(zero, own.dtype),
-        )
-        return part
-
-    pieces = gathered_once(
-        jax.tree.map(lambda part, kind: part.astype(kind), shard, (jnp.bfloat16, jnp.bfloat16)),
-        axis,
-    )
-    return combined_pairwise(jax.tree.map(kept, pieces, identity, shard), combine)
-
-
-def rms_scale(values, gain_row):
-    return (
-        values * lax.rsqrt(jnp.mean(values * values, axis=-1, keepdims=True) + EPSILON) * gain_row
-    )
-
-
-def join_states(earlier, later):
-    fade_one, state_one = earlier
-    fade_two, state_two = later
-    return (fade_one * fade_two, fade_two[..., None] * state_one + state_two)
-
-
-def advance(running_state, inputs_pair):
-    fade_now, grow_now = inputs_pair
-    return (fade_now[..., None] * running_state + grow_now, running_state)
-
-
-def shards(
-    query_matrix,
-    key_matrix,
-    value_matrix,
-    output_gate_rows,
-    decay_preactivation,
-    channel_decay_bias,
-    extra_log_decay,
-    head_norm_gain,
-    output_projection,
-    residual_input,
-    attention_norm_gain,
-    expert_before_gain,
-    expert_after_gain,
-    expert_gate_weight,
-    expert_up_weight,
-    expert_down_weight,
-    token_expert_index,
-    routing_weight_matrix,
-):
-    sequence_length = query_matrix.shape[0]
-    number_heads = value_matrix.shape[1] // DV
-    blocks = sequence_length // BLOCK
-    queries = query_matrix.astype(jnp.float32).reshape(
-        sequence_length, number_heads, KEY_CHANNELS
-    ) * KEY_CHANNELS ** (-0.5)
-    keys_all = key_matrix.astype(jnp.float32).reshape(sequence_length, number_heads, KEY_CHANNELS)
-    values_all = value_matrix.astype(jnp.float32).reshape(sequence_length, number_heads, DV)
-    decay_logarithm = (
-        jax.nn.log_sigmoid(decay_preactivation.astype(jnp.float32) + channel_decay_bias)
-        / DECAY_NORMALIZER
-    )
-    decay_logarithm = (
-        decay_logarithm.reshape(sequence_length, number_heads, KEY_CHANNELS)
-        + extra_log_decay[:, :, None]
-    )
-    running = jnp.cumsum(decay_logarithm, axis=0)
-    total_fade = jnp.exp(running[-1])
-    keys_to_end = keys_all * jnp.exp(running[-1] - running)
-    total_growth = jnp.einsum("thd,thv->hdv", keys_to_end, values_all, precision=HIGHEST)
-    q_blocks = queries.reshape(blocks, BLOCK, number_heads, KEY_CHANNELS)
-    k_blocks = keys_all.reshape(blocks, BLOCK, number_heads, KEY_CHANNELS)
-    v_blocks = values_all.reshape(blocks, BLOCK, number_heads, DV)
-    inside = jnp.cumsum(decay_logarithm.reshape(blocks, BLOCK, number_heads, KEY_CHANNELS), axis=1)
-    block_end = inside[:, -1:]
-    q_decayed = q_blocks * jnp.exp(inside)
-    k_inverse = k_blocks * jnp.exp(-inside)
-    k_to_end = k_blocks * jnp.exp(block_end - inside)
-    causal = jnp.tril(jnp.ones((BLOCK, BLOCK), dtype=bool))
-    scores = jnp.einsum("nihd,njhd->nhij", q_decayed, k_inverse, precision=HIGHEST)
-    scores = jnp.where(causal, scores, 0.0)
-    within = jnp.einsum("nhij,njhv->nihv", scores, v_blocks, precision=HIGHEST)
-    growth = jnp.einsum("nchd,nchv->nhdv", k_to_end, v_blocks, precision=HIGHEST)
-    fade_rows = jnp.exp(block_end[:, 0])
-    identity = (jnp.ones_like(total_fade), jnp.zeros_like(total_growth))
-    _, carried = carried_in((total_fade, total_growth), "sp", join_states, identity)
-    _, starts = lax.scan(advance, carried, (fade_rows, growth))
-    across = jnp.einsum("nchd,nhdv->nchv", q_decayed, starts, precision=HIGHEST)
-    attn = (within + across).reshape(sequence_length, number_heads, DV)
-    gate_act = jax.nn.silu(
-        output_gate_rows.astype(jnp.float32).reshape(sequence_length, number_heads, DV)
-    )
-    gated = (
-        (rms_scale(attn, head_norm_gain) * gate_act)
-        .astype(jnp.bfloat16)
-        .reshape(sequence_length, number_heads * DV)
-    )
-    return layer_tail(
-        gated, output_projection, residual_input, attention_norm_gain, expert_before_gain, expert_after_gain,
-        expert_gate_weight, expert_up_weight, expert_down_weight, token_expert_index, routing_weight_matrix,
+        query.T, key.T, value, gate_rows, decay.T, bias[None], extra.T, head_gain[None],
+        output_projection, residual, attention_gain[None], before_gain[None], after_gain[None],
+        w_gate[0], w_up[0], w_down[0], ids.T, weights.T,
     )
 
 

time: 139 us -> 113 us (0.81)
  Pallas kernels: 97.1 us -> 112 us
  starting transfers between devices: 13.7 us -> 0 us
  waiting for transfers between devices: 13.6 us -> 0 us
  local copies, waits for them, and re-layouts: 8.56 us -> 1.47 us
  other arithmetic: 3.81 us -> 0 us
    pallas_call x1, Pallas kernels: 97.1 us -> 112 us  [shards(): pl.pallas_call(functools.partial(layer_kernel, n_sp, n_tp, X, cap), out_s...]
    all_to_all x1 -> x0, starting transfers between devices: 13.7 us -> none  [copy_for_each(): lax.all_to_all(jnp.broadcast_to(shard[None], (peers, *shard.shape)), axis...]
    all_to_all x1 -> x0, waiting for transfers between devices: 13.6 us -> none  [copy_for_each(): lax.all_to_all(jnp.broadcast_to(shard[None], (peers, *shard.shape)), axis...]
    unnamed x22 -> x1, local copies, waits for them, and re-layouts: 5.68 us -> 1.47 us
    add x9 -> x0, other arithmetic: 1.72 us -> none  [the longest x1 0.87 us: shards(): decay_logarithm.reshape(sequence_length, number_heads, KEY_CHANNELS)]
  transfers between devices with their start and end apart: 1 -> 0, of which waited for: 1 -> 0; matrix products, arithmetic and copies ran while one was open for 2% -> 0% of each run, Pallas kernels for 0% -> 0%
where the time goes in v2:
time: 113 us
  Pallas kernels  112 us (99%)
  local copies, waits for them, and re-layouts  1.47 us (1%)
    pallas_call x1, Pallas kernels, shards(): pl.pallas_call(functools.partial(layer_kernel, n_sp, n_tp, X, cap), out_s...  112 us

profile of v2, /device:TPU:1, one launch (start us, length us, event | category | flops | bytes accessed | tf_op | source)
XLA Modules:
  0.0 113.1 jit_solution(3259786500903823322)
XLA Ops:
  0.0 111.6 %layer.1 = bf16[16,2048]{1,0:T(8,128)(2,1)} custom-call(bf16[64,256]{1,0:T(8,128)(2,1)} %bitcast.17, bf16[64,256]{1,0:T(8,128)(2,1)} %bitcast.18, bf16[256,128]{1,0:T(8,128)(2,1)} %values.1, bf16[256,128]{1,0:T(8,128)(2,1)} %gate_rows.1, bf16[64,256]{1,0:T(8,128)(2,1)} %bitcast.19, f32[1,64]{1,0:T(1,128)} %bitcast.26, f32[1,256]{1,0:T(1,128)} %bitcast.25, ...), custom_call_target="tpu_custom_call" | custom-call | tf_op jit(solution)/shard_map/layer/pallas_call | solution.py:623
  111.6 1.5 %copy.20 = bf16[16,2048]{1,0:T(8,128)(2,1)} copy(bf16[16,2048]{1,0:T(8,128)(2,1)} %layer.1) | data formatting | bytes 131072

commit v3 on v2

--- a/solution.py
+++ b/solution.py
@@ -1,4 +1,3 @@
-import contextlib
 import functools
 
 import jax
@@ -20,11 +19,7 @@
 MESH = pl.DeviceIdType.MESH
 BF16 = jnp.bfloat16
 F32 = jnp.float32
-PROFILE = False
-
-
-def scope(name):
-    return jax.named_scope(name) if PROFILE else contextlib.nullcontext()
+PARTS = 4
 
 
 def dot(a, b):
@@ -54,46 +49,63 @@
     )
 
 
-def ring_index(way, step, half, steps):
-    return way * (2 * steps - 1) + (0 if step == 1 else 1 + (step - 2) * 2 + half)
-
-
-def ring_sum(at, part, out, sends, recvs, send_sems, recv_sems):
+def ring_index(way, step, part, steps):
+    first = part % (PARTS // 2) if step == 1 else PARTS // 2 + (step - 2) * PARTS + part
+    return way * ring_size(steps) + first
+
+
+def ring_size(steps):
+    return PARTS // 2 + (steps - 1) * PARTS
+
+
+def way_parts(way):
+    low, high = list(range(PARTS // 2)), list(range(PARTS // 2, PARTS))
+    return (low, high) if way == 0 else (high, low)
+
+
+def both_ways(pick):
+    return [(way, part) for pair in zip(pick(0), pick(1)) for way, part in enumerate(pair)]
+
+
+def whole(ref, sem):
+    return pltpu.make_async_copy(ref, ref, sem)
+
+
+def ring_sum(at, part_of, out, sends, recvs, send_sem, recv_sems):
     Y, steps, y = at.Y, at.Y // 2, at.y
 
-    def copy(way, step, half):
-        i = ring_index(way, step, half, steps)
+    def copy(way, step, part):
+        i = ring_index(way, step, part, steps)
         to = (y + 1) % Y if way == 0 else (y + Y - 1) % Y
-        return remote(sends.at[i], recvs.at[i], send_sems.at[i], recv_sems.at[i], at.at(y=to))
+        return remote(sends.at[i], recvs.at[i], send_sem, recv_sems.at[i], at.at(y=to))
 
     def offset(way, step):
         k = steps - step + 1
         return k if way == 0 or k == steps else -k
 
-    started = []
-
-    def send(way, step, half, value):
-        sends[ring_index(way, step, half, steps)] = value.astype(BF16)
-        c = copy(way, step, half)
-        c.start()
-        started.append(c)
-
-    for way, half in ((0, 0), (1, 1)):
-        send(way, 1, half, part(offset(way, 1), half))
+    def send(way, step, part, value):
+        sends[ring_index(way, step, part, steps)] = value.astype(BF16)
+        copy(way, step, part).start()
+
+    for way, part in both_ways(lambda w: way_parts(w)[0]):
+        send(way, 1, part, part_of(offset(way, 1), part))
     for step in range(2, steps + 1):
-        for way, half in ((0, 1), (1, 0), (0, 0), (1, 1)):
-            value = part(offset(way, step), half)
-            if step > 2 or way == half:
-                copy(way, step - 1, half).wait_recv()
-                value = value + recvs[ring_index(way, step - 1, half, steps)].astype(F32)
-            send(way, step, half, value)
-    for half in (0, 1):
-        total = part(0, half)
+        for way, part in both_ways(lambda w: way_parts(w)[1] + way_parts(w)[0]):
+            value = part_of(offset(way, step), part)
+            if step > 2 or part in way_parts(way)[0]:
+                copy(way, step - 1, part).wait_recv()
+                value = value + recvs[ring_index(way, step - 1, part, steps)].astype(F32)
+            send(way, step, part, value)
+    for part in range(PARTS):
+        total = part_of(0, part)
         for way in (0, 1):
-            copy(way, steps, half).wait_recv()
-            total = total + recvs[ring_index(way, steps, half, steps)].astype(F32)
-        out(half, total)
-    return started
+            copy(way, steps, part).wait_recv()
+            total = total + recvs[ring_index(way, steps, part, steps)].astype(F32)
+        out(part, total)
+
+
+def far_first(count):
+    return sorted(range(1, count), key=lambda k: (-min(k, count - k), k))
 
 
 def split(value):
@@ -117,16 +129,14 @@
 
 def layer_kernel(
     n_sp, n_tp, group, cap,
-    q_t, k_t, values, gate_rows, decay_t, bias, extra, head_gain,
-    w_out, residual, attention_gain, before_gain, after_gain,
-    w_gate, w_up, w_down, ids_row, weights_row,
+    operands, w_out, w_gate, w_up, w_down,
     out,
+    held,
     gated, stack, spread, find, turn_out, turn_back, sx, rx, sz, rz,
     gu, wd, wo, partner, mixed, mid, normed, block, rows, acc, hid, shares, result,
     zs, zr, xs, xb, zs2, zr2, column, branch,
     sa, ra, sb, rb,
-    wsem, wrs, wrr, gsem, as_, ar, zss, zrs, xss, xrs, gs, gr, bs, br, xbs, xbr, zbs, zbr, fs,
-    sxs, sxr, szs, szr,
+    wsem, wrs, wrr, gsem, sums, gr, xrs, xbs, szs, szr, osem, done, came,
 ):
     at = Place(n_sp, n_tp, group)
     X, Y, Z, C = at.X, at.Y, at.Z, at.C
@@ -134,16 +144,19 @@
     steps = Y // 2
     other = 1 - c
 
+    (
+        q_t, k_t, values, gate_rows, decay_t, bias, extra, head_gain,
+        residual, attention_gain, before_gain, after_gain, ids_row, weights_row,
+    ) = held
+    loads = [pltpu.make_async_copy(a, b, osem.at[k]) for k, (a, b) in enumerate(zip(operands, held))]
+    for k in loads:
+        k.start()
     local = [
         pltpu.make_async_copy(w_gate, gu.at[0], wsem.at[0]),
         pltpu.make_async_copy(w_up, gu.at[1], wsem.at[1]),
         pltpu.make_async_copy(w_down, wd.at[0], wsem.at[2]),
         pltpu.make_async_copy(w_out, wo.at[0], wsem.at[3]),
     ]
-    local[3].start()
-    for k in (0, 1, 2):
-        local[k].start()
-
     rz[...] = jnp.zeros_like(rz)
     barrier = pltpu.get_barrier_semaphore()
 
@@ -157,6 +170,11 @@
     for k in range(1, X):
         for core in range(C):
             pl.semaphore_signal(barrier, inc=1, device_id=at.at(x=(x + k) % X, c=core), device_id_type=MESH)
+
+    for k in (3, 0, 1, 2):
+        local[k].start()
+    for k in loads:
+        k.wait()
 
     tokens = q_t.shape[1]
     blocks = tokens // BLOCK
@@ -188,7 +206,7 @@
     pl.semaphore_wait(barrier, n_tp - 1 + Z - 1 + (X - 1) * C)
 
     def state_x(k):
-        return remote(sx, rx.at[x], sxs.at[k], sxr.at[k], at.at(x=(x + k) % X))
+        return remote(sx, rx.at[x], done.at[7], came.at[4], at.at(x=(x + k) % X))
 
     for k in range(1, X):
         state_x(k).start()
@@ -226,8 +244,7 @@
     scores = jnp.where((r >= q) & one_block, scores, 0.0).astype(BF16)
     within = dot(scores, vals)
 
-    for k in range(1, X):
-        state_x(k).wait_recv()
+    whole(rx.at[pl.ds(0, X - 1)], came.at[4]).wait()
     plane, plane_row = rx[0, 0:KEY_CHANNELS].astype(F32), rx[0, KEY_CHANNELS:tail][0:1].astype(F32)
     ahead, ahead_fade = jnp.zeros_like(state), jnp.ones((KEY_CHANNELS, 1), F32)
     for k in range(X):
@@ -303,18 +320,18 @@
         value = dot(mine, wo[0, :, cols]) + dot(theirs, wo[1, :, cols])
         mixed[:, :, cols] = value.reshape(share, piece, tile)
 
-    half_width = width // 2
-
-    def mixed_part(k, half):
+    part_width = width // PARTS
+
+    def mixed_part(k, part):
         d = (y + k + Y) % Y
-        return mixed[pl.ds(d, 1), :, half * half_width : (half + 1) * half_width].reshape(piece, half_width)
-
-    total = [None, None]
-
-    def keep(half, value):
-        total[half] = value
-
-    sum_a = ring_sum(at, mixed_part, keep, sa, ra, as_.at[0], as_.at[1])
+        return mixed[pl.ds(d, 1), :, part * part_width : (part + 1) * part_width].reshape(piece, part_width)
+
+    total = [None] * PARTS
+
+    def keep(part, value):
+        total[part] = value
+
+    ring_sum(at, mixed_part, keep, sa, ra, done.at[0], sums)
     attn = jnp.concatenate(total, axis=1)
     attn = attn * lax.rsqrt(jnp.mean(attn * attn, axis=1, keepdims=True) + EPSILON) * attention_gain[...]
     mid[...] = (residual[...].astype(F32) + attn).astype(BF16)
@@ -331,45 +348,42 @@
     def to_width(k):
         t = (at.tp + k) % n_tp
         return remote(
-            normed.at[:, share_cols(t)], block.at[share_rows(at.tp), :], ar.at[0, k], ar.at[1, k], (at.sp, t)
+            normed.at[:, share_cols(t)], block.at[share_rows(at.tp), :], done.at[3], came.at[0], (at.sp, t)
         )
 
     def start_width(k, carry):
         to_width(k).start()
         return carry
 
-    def wait_width(k, carry):
-        to_width(k).wait_recv()
-        return carry
-
     lax.fori_loop(1, n_tp, start_width, 0)
     block[share_rows(at.tp), :] = normed[:, share_cols(at.tp)]
 
-    lax.fori_loop(1, n_tp, wait_width, 0)
+    others = block.at[pl.ds(0, (n_tp - 1) * piece)]
+    whole(others, came.at[0]).wait()
     picked = dot(spread[...], block[...]).astype(BF16)
     zs[...] = picked.reshape(zs.shape)
 
     def z_out(k):
-        return remote(zs.at[(z + k) % Z], zr.at[z], zss.at[k], zrs.at[k], at.at(z=(z + k) % Z))
-
-    for k in range(1, Z):
+        return remote(zs.at[(z + k) % Z], zr.at[z], done.at[5], came.at[2], at.at(z=(z + k) % Z))
+
+    for k in far_first(Z):
         z_out(k).start()
     zr[pl.ds(z, 1)] = zs[pl.ds(z, 1)]
-    for k in range(1, Z):
-        z_out(k).wait_recv()
+    whole(zr.at[pl.ds(0, Z - 1)], came.at[2]).wait()
 
     xs[...] = dot(turn_out[...], zr[...].reshape(slots, DV)).astype(BF16).reshape(xs.shape)
 
     side = x % C
     mine_half = x // C
+    per = PARTS // 2
 
     def x_out(k):
         to = (x + k) % X
         return (
             xs.at[to],
-            rows.at[y, mine_half, :, share_cols(c)],
-            xss.at[k],
-            xrs.at[mine_half, c],
+            rows.at[y, pl.ds(mine_half * per, per), :, share_cols(c)],
+            done.at[8 if k else 9],
+            xrs.at[mine_half],
             at.at(x=to, c=side),
         )
 
@@ -385,24 +399,20 @@
     def _():
         remote(src, dst, s_sem, r_sem, pair).start()
 
-    def gather(way, step, half):
+    def gather(way, step, part):
         j = (y + Y - (step - 1)) % Y if way == 0 else (y + step - 1) % Y
         to = (y + 1) % Y if way == 0 else (y + Y - 1) % Y
-        i = way * (2 * steps - 1) + (step - 1) * 2 + (half if step < steps else 0)
-        return remote(rows.at[j, half], rows.at[j, half], gs.at[i], gr.at[i], at.at(y=to))
-
-    gathers = []
-
-    def start_gather(way, step, half):
-        g = gather(way, step, half)
-        g.start()
-        gathers.append(g)
+        i = way * ring_size(steps) + (step - 1) * PARTS + (part if step < steps else part % per)
+        return remote(rows.at[j, part], rows.at[j, part], done.at[2], gr.at[i], at.at(y=to))
+
+    def start_gather(way, step, part):
+        gather(way, step, part).start()
 
     for half in (0, 1):
-        for core in range(C):
-            pltpu.make_async_copy(xs.at[0], rows.at[y, half, :, pl.ds(core * DV, DV)], xrs.at[half, core]).wait()
-        for way in (0, 1):
-            start_gather(way, 1, half)
+        whole(rows.at[y, pl.ds(half * per, per)], xrs.at[half]).wait()
+        for part in range(half * per, half * per + per):
+            for way in (0, 1):
+                start_gather(way, 1, part)
 
     count = rows.shape[1] * rows.shape[2]
     chunk = rows.shape[3]
@@ -420,15 +430,15 @@
 
     grow(y, True)
     for step in range(1, steps):
-        for half in (0, 1):
+        for part in range(PARTS):
             for way in (0, 1):
-                gather(way, step, half).wait_recv()
-                if step + 1 < steps or way == half:
-                    start_gather(way, step + 1, half)
+                gather(way, step, part).wait_recv()
+                if step + 1 < steps or way == part // per:
+                    start_gather(way, step + 1, part)
         grow((y + Y - step) % Y)
         grow((y + step) % Y)
-    for way in (0, 1):
-        gather(way, steps, way).wait_recv()
+    for part in range(PARTS):
+        gather(part // per, steps, part).wait_recv()
     grow((y + steps) % Y)
 
     for k in (0, 1):
@@ -443,32 +453,30 @@
         d = (y + offset + Y) % Y
         cols = pl.ds(pl.multiple_of(d * chunk, chunk), chunk)
         value = dot(hid[0], wd[0, :, cols]) + dot(hid[1], wd[1, :, cols])
-        shares[offset + steps - 1] = value.reshape(2, count // 2, chunk)
-
-    def down_part(offset, half):
+        shares[offset + steps - 1] = value.reshape(PARTS, count // PARTS, chunk)
+
+    def down_part(offset, part):
         if offset not in made:
             down(offset)
             made[offset] = True
-        return shares[offset + steps - 1, half]
-
-    def keep_result(half, value):
-        result[half] = value.astype(BF16)
-
-    sum_b = ring_sum(at, down_part, keep_result, sb, rb, bs, br)
+        return shares[offset + steps - 1, part]
 
     def x_back(half, core):
         home = 2 * half + c
         return (
-            result.at[half, :, pl.ds(core * DV, DV)],
+            result.at[pl.ds(half * per, per), :, pl.ds(core * DV, DV)],
             xb.at[x],
             xbs.at[2 * half + core],
-            xbr.at[x],
+            came.at[5],
             at.at(x=home, c=core),
         ), (home == x) & (c == core)
 
-    for half in (0, 1):
+    def keep_result(part, value):
+        result[part] = value.astype(BF16)
+        if part % per < per - 1:
+            return
         for core in range(C):
-            args, here = x_back(half, core)
+            args, here = x_back(part // per, core)
 
             @pl.when(here)
             def _(args=args):
@@ -478,18 +486,18 @@
             def _(args=args):
                 remote(*args).start()
 
-    for k in range(X):
-        pltpu.make_async_copy(xs.at[0], xb.at[k], xbr.at[k]).wait()
+    ring_sum(at, down_part, keep_result, sb, rb, done.at[1], sums)
+
+    whole(xb, came.at[5]).wait()
     zs2[...] = dot(turn_back[...], xb[...].reshape(slots, DV)).astype(BF16).reshape(zs2.shape)
 
     def z_back(k):
-        return remote(zs2.at[(z + k) % Z], zr2.at[z], zbs.at[k], zbr.at[k], at.at(z=(z + k) % Z))
-
-    for k in range(1, Z):
+        return remote(zs2.at[(z + k) % Z], zr2.at[z], done.at[6], came.at[3], at.at(z=(z + k) % Z))
+
+    for k in far_first(Z):
         z_back(k).start()
     zr2[pl.ds(z, 1)] = zs2[pl.ds(z, 1)]
-    for k in range(1, Z):
-        z_back(k).wait_recv()
+    whole(zr2.at[pl.ds(0, Z - 1)], came.at[3]).wait()
     lookup = zr2[...].reshape(slots, DV)
     column[...] = (
         weight_cols[0] * dot(find[0], lookup) + weight_cols[1] * dot(find[1], lookup)
@@ -498,26 +506,21 @@
     def to_rows(k):
         t = (at.tp + k) % n_tp
         return remote(
-            column.at[share_rows(t), :], branch.at[:, share_cols(at.tp)], fs.at[0, k], fs.at[1, k], (at.sp, t)
+            column.at[share_rows(t), :], branch.at[:, share_cols(at.tp)], done.at[4], came.at[1], (at.sp, t)
         )
 
     def start_rows(k, carry):
         to_rows(k).start()
         return carry
 
-    def wait_rows(k, carry):
-        to_rows(k).wait_recv()
-        return carry
-
     lax.fori_loop(1, n_tp, start_rows, 0)
     branch[:, share_cols(at.tp)] = column[share_rows(at.tp), :]
-    lax.fori_loop(1, n_tp, wait_rows, 0)
+    whole(others, came.at[1]).wait()
     b = branch[...].astype(F32)
     b = b * lax.rsqrt(jnp.mean(b * b, axis=1, keepdims=True) + EPSILON) * after_gain[...]
     out[...] = (mid[...].astype(F32) + b).astype(BF16)
 
-    for k in range(1, X):
-        state_x(k).wait_send()
+    whole(rx.at[pl.ds(0, X - 1)], done.at[7]).wait()
     for k in range(1, Z):
 
         @pl.when(z + k < Z)
@@ -525,20 +528,16 @@
             state_z(k).wait_send()
 
     swap.wait_send()
-    for k in crossed + sum_a + gathers + sum_b:
+    for k in crossed:
         k.wait_send()
-
-    def wait_sent(k, carry):
-        to_width(k).wait_send()
-        to_rows(k).wait_send()
-        return carry
-
-    lax.fori_loop(1, n_tp, wait_sent, 0)
-    for k in range(1, Z):
-        z_out(k).wait_send()
-        z_back(k).wait_send()
-    for k in range(1, X):
-        remote(*x_out(k)).wait_send()
+    whole(sa, done.at[0]).wait()
+    whole(sb, done.at[1]).wait()
+    whole(rows.at[pl.ds(0, Y - 1)], done.at[2]).wait()
+    whole(others, done.at[3]).wait()
+    whole(others, done.at[4]).wait()
+    whole(zr.at[pl.ds(0, Z - 1)], done.at[5]).wait()
+    whole(zr2.at[pl.ds(0, Z - 1)], done.at[6]).wait()
+    whole(xs.at[pl.ds(0, X - 1)], done.at[8]).wait()
 
     @pl.when(side != c)
     def _():
@@ -565,14 +564,19 @@
     cap = 5 * tokens // (2 * n_sp)
     slots = n_sp * cap
     steps = Y // 2
-    msgs = 2 * (2 * steps - 1)
-    half = slots // 4
+    msgs = 2 * ring_size(steps)
+    part = slots // C // PARTS
     chunk = C * DV
     hidden = w_gate.shape[2]
-    vm, hbm = pl.BlockSpec(memory_space=pltpu.VMEM), pl.BlockSpec(memory_space=pl.ANY)
+    hbm = pl.BlockSpec(memory_space=pltpu.HBM)
     sem = pltpu.SemaphoreType.DMA
     message = (KEY_CHANNELS + 16, DV)
+    operands = [
+        query.T, key.T, value, gate_rows, decay.T, bias[None], extra.T, head_gain[None],
+        residual, attention_gain[None], before_gain[None], after_gain[None], ids.T, weights.T,
+    ]
     scratch = [
+        [pltpu.VMEM(a.shape, a.dtype) for a in operands],
         pltpu.VMEM((Y, C, piece, DV), BF16),
         pltpu.VMEM((128, tokens), F32),
         pltpu.VMEM((slots, tokens), BF16),
@@ -591,49 +595,38 @@
         pltpu.VMEM((piece, width), BF16),
         pltpu.VMEM((piece, width), BF16),
         pltpu.VMEM((tokens, DV), BF16),
-        pltpu.VMEM((Y, 2, half, chunk), BF16),
-        pltpu.VMEM((4, 2 * half, hidden), F32),
-        pltpu.VMEM((2, 2 * half, hidden), BF16),
-        pltpu.VMEM((Y, 2, half, chunk), F32),
-        pltpu.VMEM((2, half, chunk), BF16),
+        pltpu.VMEM((Y, PARTS, part, chunk), BF16),
+        pltpu.VMEM((4, PARTS * part, hidden), F32),
+        pltpu.VMEM((2, PARTS * part, hidden), BF16),
+        pltpu.VMEM((Y, PARTS, part, chunk), F32),
+        pltpu.VMEM((PARTS, part, chunk), BF16),
         pltpu.VMEM((Z, X * cap, DV), BF16),
         pltpu.VMEM((Z, X * cap, DV), BF16),
-        pltpu.VMEM((X, Z * cap, DV), BF16),
-        pltpu.VMEM((X, Z * cap, DV), BF16),
+        pltpu.VMEM((X, PARTS // 2, part, DV), BF16),
+        pltpu.VMEM((X, PARTS // 2, part, DV), BF16),
         pltpu.VMEM((Z, X * cap, DV), BF16),
         pltpu.VMEM((Z, X * cap, DV), BF16),
         pltpu.VMEM((tokens, DV), BF16),
         pltpu.VMEM((piece, width), BF16),
-        pltpu.VMEM((msgs, piece, width // 2), BF16),
-        pltpu.VMEM((msgs, piece, width // 2), BF16),
-        pltpu.VMEM((msgs, half, chunk), BF16),
-        pltpu.VMEM((msgs, half, chunk), BF16),
-        sem((4,)), sem((4,)), sem((4,)), sem((2,)),
-        sem((2, msgs)),
-        sem((2, n_tp)),
-        sem((Z,)), sem((Z,)),
-        sem((X,)), sem((2, C)),
-        sem((msgs,)), sem((msgs,)),
-        sem((msgs,)), sem((msgs,)),
-        sem((2 * C,)), sem((X,)),
-        sem((Z,)), sem((Z,)),
-        sem((2, n_tp)),
-        sem((X,)), sem((X,)), sem((Z,)), sem((Z,)),
+        pltpu.VMEM((msgs, piece, width // PARTS), BF16),
+        pltpu.VMEM((msgs, piece, width // PARTS), BF16),
+        pltpu.VMEM((msgs, part, chunk), BF16),
+        pltpu.VMEM((msgs, part, chunk), BF16),
+        sem((4,)), sem((4,)), sem((4,)), sem((2,)), sem((msgs,)), sem((msgs,)), sem((2,)), sem((2 * C,)),
+        sem((Z,)), sem((Z,)), sem((len(operands),)), sem((10,)), sem((6,)),
     ]
     return pl.pallas_call(
         functools.partial(layer_kernel, n_sp, n_tp, X, cap),
         out_shape=jax.ShapeDtypeStruct((piece, width), BF16),
-        in_specs=[vm] * 8 + [hbm] + [vm] * 4 + [hbm] * 3 + [vm] * 2,
-        out_specs=vm,
+        in_specs=[[hbm] * len(operands), hbm, hbm, hbm, hbm],
+        out_specs=pl.BlockSpec(memory_space=pltpu.VMEM),
         scratch_shapes=scratch,
         name="layer",
         compiler_params=pltpu.CompilerParams(
-            collective_id=0, has_side_effects=True, vmem_limit_bytes=60 * 1024 * 1024
+            collective_id=0, has_side_effects=True, vmem_limit_bytes=40 * 1024 * 1024
         ),
     )(
-        query.T, key.T, value, gate_rows, decay.T, bias[None], extra.T, head_gain[None],
-        output_projection, residual, attention_gain[None], before_gain[None], after_gain[None],
-        w_gate[0], w_up[0], w_down[0], ids.T, weights.T,
+        *jax.tree.map(lambda a: pltpu.with_memory_space_constraint(a, pltpu.HBM), (operands, output_projection, w_gate[0], w_up[0], w_down[0]))
     )
 
 

time: 113 us -> 106 us (0.938)
  Pallas kernels: 112 us -> 105 us
    pallas_call x1, Pallas kernels: 112 us -> 105 us  [shards(): pl.pallas_call(functools.partial(layer_kernel, n_sp, n_tp, X, cap), out_s...]
where the time goes in v3:
time: 106 us
  Pallas kernels  105 us (99%)
    pallas_call x1, Pallas kernels, shards(): pl.pallas_call(functools.partial(layer_kernel, n_sp, n_tp, X, cap), out_s...  105 us

profile of v3, /device:TPU:1, one launch (start us, length us, event | category | flops | bytes accessed | tf_op | source)
XLA Modules:
  0.0 105.8 jit_solution(10246874251841030614)
XLA Ops:
  0.0 105.1 %layer.1 = bf16[16,2048]{1,0:T(8,128)(2,1)S(1)} custom-call(bf16[64,256]{1,0:T(8,128)(2,1)} %bitcast.17, bf16[64,256]{1,0:T(8,128)(2,1)} %bitcast.18, bf16[256,128]{1,0:T(8,128)(2,1)} %operands_2_.1, bf16[256,128]{1,0:T(8,128)(2,1)} %operands_3_.1, bf16[64,256]{1,0:T(8,128)(2,1)} %bitcast.19, f32[1,64]{1,0:T(1,128)} %bitcast.26, f32[1,256]{1,0:T(1,128)} %bitcast.25, ...), custom_call_target="tpu_custom_call" | custom-call | tf_op jit(solution)/shard_map/layer/pallas_call | solution.py:618
  105.1 0.6 copy.20

commit v4 on v3

--- a/solution.py
+++ b/solution.py
@@ -132,8 +132,8 @@
     operands, w_out, w_gate, w_up, w_down,
     out,
     held,
-    gated, stack, spread, find, turn_out, turn_back, sx, rx, sz, rz,
-    gu, wd, wo, partner, mixed, mid, normed, block, rows, acc, hid, shares, result,
+    gated, stack, facts, spread, find, told, heard, serve, merge, sx, rx, sz, rz,
+    gu, wd, wo, partner, mixed, summed, mid, normed, block, rows, acc, hid, shares, result,
     zs, zr, xs, xb, zs2, zr2, column, branch,
     sa, ra, sb, rb,
     wsem, wrs, wrr, gsem, sums, gr, xrs, xbs, szs, szr, osem, done, came,
@@ -222,24 +222,31 @@
     rx[pl.ds(x, 1)] = sx[...].reshape(1, tail, DV)
 
     slots = n_sp * cap
+    seats = zs.shape[1]
     sub = lax.broadcasted_iota(jnp.int32, (n_sp, tokens), 0)
     chosen = [ids_row[k : k + 1, :] for k in range(TOP)]
     named = jnp.where((sub == chosen[0]) | (sub == chosen[1]), 1.0, 0.0).astype(BF16)
     before = dot(named, jnp.where(r < q, 1.0, 0.0).astype(BF16))
     targets = []
+    plane_of = chosen[0] // X
     for e in chosen:
         slot = jnp.sum(jnp.where(sub == e, before, 0.0), axis=0, keepdims=True)
-        targets.append(e * cap + slot.astype(jnp.int32))
+        targets.append((e - plane_of * X) * (Z * cap) + z * cap + slot.astype(jnp.int32))
+    sub = lax.broadcasted_iota(jnp.int32, (Z, tokens), 0)
+    before = dot(jnp.where(sub == plane_of, 1.0, 0.0).astype(BF16), jnp.where(r < q, 1.0, 0.0).astype(BF16))
+    rank = jnp.sum(jnp.where(sub == plane_of, before, 0.0), axis=0, keepdims=True)
+    seat = plane_of * seats + rank.astype(jnp.int32)
     query = q_t[...].astype(F32) * (KEY_CHANNELS**-0.5 * jnp.exp(inside))
     stack[0:KEY_CHANNELS, :] = query
     stack[KEY_CHANNELS:, :] = jnp.zeros((stack.shape[0] - KEY_CHANNELS, tokens), F32)
+    stack[KEY_CHANNELS : KEY_CHANNELS + 1, :] = seat.astype(F32)
+    facts[...] = jnp.zeros_like(facts)
     for k in range(TOP):
-        stack[KEY_CHANNELS + k : KEY_CHANNELS + k + 1, :] = targets[k].astype(F32)
-        stack[KEY_CHANNELS + TOP + k : KEY_CHANNELS + TOP + k + 1, :] = weights_row[k : k + 1, :]
+        facts[k : k + 1, :] = (targets[k] + 1).astype(F32)
+        facts[TOP + k : TOP + k + 1, :] = weights_row[k : k + 1, :]
     stood = stack[...].T
     query = stood[:, 0:KEY_CHANNELS].astype(BF16)
-    target_cols = [stood[:, KEY_CHANNELS + k : KEY_CHANNELS + k + 1].astype(jnp.int32) for k in range(TOP)]
-    weight_cols = [stood[:, KEY_CHANNELS + TOP + k : KEY_CHANNELS + TOP + k + 1] for k in range(TOP)]
+    seat_col = stood[:, KEY_CHANNELS : KEY_CHANNELS + 1].astype(jnp.int32)
     scores = dot(query, (keys * jnp.exp(-inside)).astype(BF16))
     scores = jnp.where((r >= q) & one_block, scores, 0.0).astype(BF16)
     within = dot(scores, vals)
@@ -265,23 +272,23 @@
         def _(k=k):
             state_z(k).start()
 
-    tall = lax.broadcasted_iota(jnp.int32, (slots, tokens), 0)
-    hits = [jnp.where(tall == t, 1.0, 0.0) for t in targets]
-    spread[...] = (hits[0] + hits[1]).astype(BF16)
-    wide = lax.broadcasted_iota(jnp.int32, (tokens, slots), 1)
-    for k in range(TOP):
-        find[k] = jnp.where(wide == target_cols[k], 1.0, 0.0).astype(BF16)
-    lane = lax.broadcasted_iota(jnp.int32, (1, slots), 1)
-
-    def turned(outer, inner):
-        a = sum(jnp.where(lane >= k * inner * cap, 1, 0) for k in range(1, outer))
-        rest = lane - a * (inner * cap)
-        b = sum(jnp.where(rest >= k * cap, 1, 0) for k in range(1, inner))
-        return b * (outer * cap) + a * cap + (rest - b * cap)
-
-    down_rows = lax.broadcasted_iota(jnp.int32, (slots, slots), 0)
-    turn_out[...] = jnp.where(down_rows == turned(Z, X), 1.0, 0.0).astype(BF16)
-    turn_back[...] = jnp.where(down_rows == turned(X, Z), 1.0, 0.0).astype(BF16)
+    all_seats = Z * seats
+    tall = lax.broadcasted_iota(jnp.int32, (all_seats, tokens), 0)
+    spread[...] = jnp.where(tall == seat, 1.0, 0.0).astype(BF16)
+    wide = lax.broadcasted_iota(jnp.int32, (tokens, all_seats), 1)
+    find[...] = jnp.where(wide == seat_col, 1.0, 0.0).astype(BF16)
+    listed = sum(dot(term, find[...]) for term in split(facts[...]))
+    near = lax.broadcasted_iota(jnp.int32, (8, DV), 1) < seats
+    for k in range(Z):
+        moved = pltpu.roll(listed, (all_seats - k * seats) % all_seats, 1) if k else listed
+        told[k] = jnp.where(near, moved[:, 0:DV], 0.0)
+
+    def tell(k):
+        return remote(told.at[(z + k) % Z], heard.at[z], done.at[10], came.at[6], at.at(z=(z + k) % Z))
+
+    for k in far_first(Z):
+        tell(k).start()
+    heard[pl.ds(z, 1)] = told[pl.ds(z, 1)]
     gate_act = gate_rows[...].astype(F32)
     gate_act = gate_act * jax.nn.sigmoid(gate_act) * head_gain[...]
 
@@ -303,36 +310,45 @@
     heads = within + jnp.concatenate(across, axis=0)
     heads = heads * lax.rsqrt(jnp.mean(heads * heads, axis=1, keepdims=True) + EPSILON) * gate_act
     gated[...] = heads.astype(BF16).reshape(gated.shape)
-    swap = remote(gated.at[:, other], partner, gsem.at[0], gsem.at[1], pair)
-    swap.start()
-
-    share = gated.shape[0]
+    lead = c == C - 1
+    swap = remote(gated, partner, gsem.at[0], gsem.at[1], pair)
+
+    @pl.when(jnp.logical_not(lead))
+    def _():
+        swap.start()
+
+
     piece = gated.shape[2]
     width = wo.shape[2]
-    swap.wait_recv()
     local[3].wait()
     crossed[0].wait_recv()
-    mine = gated[:, pl.ds(c, 1)].reshape(share * piece, DV)
-    theirs = partner[...].reshape(share * piece, DV)
-    tile = width // 4
-    for k in range(4):
-        cols = slice(k * tile, (k + 1) * tile)
-        value = dot(mine, wo[0, :, cols]) + dot(theirs, wo[1, :, cols])
-        mixed[:, :, cols] = value.reshape(share, piece, tile)
-
     part_width = width // PARTS
+    handed = remote(summed.at[0], summed.at[0], gsem.at[2], gsem.at[3], pair)
 
     def mixed_part(k, part):
         d = (y + k + Y) % Y
-        return mixed[pl.ds(d, 1), :, part * part_width : (part + 1) * part_width].reshape(piece, part_width)
-
-    total = [None] * PARTS
+        return mixed[pl.ds(d, 1), :, part * part_width : (part + 1) * part_width].reshape(C * piece, part_width)
 
     def keep(part, value):
-        total[part] = value
-
-    ring_sum(at, mixed_part, keep, sa, ra, done.at[0], sums)
-    attn = jnp.concatenate(total, axis=1)
+        summed[:, :, part * part_width : (part + 1) * part_width] = value.reshape(C, piece, part_width)
+
+    @pl.when(lead)
+    def _():
+        swap.wait_recv()
+        mine = gated[...].reshape(tokens, DV)
+        theirs = partner[...].reshape(tokens, DV)
+        for k in range(PARTS):
+            cols = slice(k * part_width, (k + 1) * part_width)
+            value = dot(mine, wo[0, :, cols]) + dot(theirs, wo[1, :, cols])
+            mixed[:, :, cols] = value.reshape(Y, C * piece, part_width)
+        ring_sum(at, mixed_part, keep, sa, ra, done.at[0], sums)
+        handed.start()
+
+    @pl.when(jnp.logical_not(lead))
+    def _():
+        handed.wait_recv()
+
+    attn = summed[pl.ds(c, 1)].reshape(piece, width)
     attn = attn * lax.rsqrt(jnp.mean(attn * attn, axis=1, keepdims=True) + EPSILON) * attention_gain[...]
     mid[...] = (residual[...].astype(F32) + attn).astype(BF16)
     m = mid[...].astype(F32)
@@ -358,6 +374,20 @@
     lax.fori_loop(1, n_tp, start_width, 0)
     block[share_rows(at.tp), :] = normed[:, share_cols(at.tp)]
 
+    whole(heard.at[pl.ds(0, Z - 1)], came.at[6]).wait()
+    lists = None
+    for k in range(Z):
+        part = jnp.concatenate([heard[k], jnp.zeros((8, all_seats - DV), F32)], axis=1)
+        part = pltpu.roll(part, k * seats, 1) if k else part
+        lists = part if lists is None else lists + part
+    tall = lax.broadcasted_iota(jnp.int32, (slots, all_seats), 0)
+    hits = [jnp.where(tall == lists[k : k + 1, :].astype(jnp.int32) - 1, 1.0, 0.0) for k in range(TOP)]
+    serve[...] = (hits[0] + hits[1]).astype(BF16)
+    stood = jnp.concatenate([lists, jnp.zeros((DV - 8, all_seats), F32)], axis=0).T
+    wide = lax.broadcasted_iota(jnp.int32, (all_seats, slots), 1)
+    for k in range(TOP):
+        merge[k] = jnp.where(wide == stood[:, k : k + 1].astype(jnp.int32) - 1, 1.0, 0.0).astype(BF16)
+    shares_of = [stood[:, TOP + k : TOP + k + 1] for k in range(TOP)]
     others = block.at[pl.ds(0, (n_tp - 1) * piece)]
     whole(others, came.at[0]).wait()
     picked = dot(spread[...], block[...]).astype(BF16)
@@ -371,7 +401,7 @@
     zr[pl.ds(z, 1)] = zs[pl.ds(z, 1)]
     whole(zr.at[pl.ds(0, Z - 1)], came.at[2]).wait()
 
-    xs[...] = dot(turn_out[...], zr[...].reshape(slots, DV)).astype(BF16).reshape(xs.shape)
+    xs[...] = dot(serve[...], zr[...].reshape(all_seats, DV)).astype(BF16).reshape(xs.shape)
 
     side = x % C
     mine_half = x // C
@@ -489,7 +519,9 @@
     ring_sum(at, down_part, keep_result, sb, rb, done.at[1], sums)
 
     whole(xb, came.at[5]).wait()
-    zs2[...] = dot(turn_back[...], xb[...].reshape(slots, DV)).astype(BF16).reshape(zs2.shape)
+    served = xb[...].reshape(slots, DV)
+    served = shares_of[0] * dot(merge[0], served) + shares_of[1] * dot(merge[1], served)
+    zs2[...] = served.astype(BF16).reshape(zs2.shape)
 
     def z_back(k):
         return remote(zs2.at[(z + k) % Z], zr2.at[z], done.at[6], came.at[3], at.at(z=(z + k) % Z))
@@ -498,10 +530,7 @@
         z_back(k).start()
     zr2[pl.ds(z, 1)] = zs2[pl.ds(z, 1)]
     whole(zr2.at[pl.ds(0, Z - 1)], came.at[3]).wait()
-    lookup = zr2[...].reshape(slots, DV)
-    column[...] = (
-        weight_cols[0] * dot(find[0], lookup) + weight_cols[1] * dot(find[1], lookup)
-    ).astype(BF16)
+    column[...] = dot(find[...], zr2[...].reshape(all_seats, DV)).astype(BF16)
 
     def to_rows(k):
         t = (at.tp + k) % n_tp
@@ -527,15 +556,23 @@
         def _(k=k):
             state_z(k).wait_send()
 
-    swap.wait_send()
+    @pl.when(jnp.logical_not(lead))
+    def _():
+        swap.wait_send()
+
+    @pl.when(lead)
+    def _():
+        handed.wait_send()
+        whole(sa, done.at[0]).wait()
+
     for k in crossed:
         k.wait_send()
-    whole(sa, done.at[0]).wait()
     whole(sb, done.at[1]).wait()
     whole(rows.at[pl.ds(0, Y - 1)], done.at[2]).wait()
     whole(others, done.at[3]).wait()
     whole(others, done.at[4]).wait()
     whole(zr.at[pl.ds(0, Z - 1)], done.at[5]).wait()
+    whole(told.at[pl.ds(0, Z - 1)], done.at[10]).wait()
     whole(zr2.at[pl.ds(0, Z - 1)], done.at[6]).wait()
     whole(xs.at[pl.ds(0, X - 1)], done.at[8]).wait()
 
@@ -563,6 +600,7 @@
     Z, Y = n_sp // X, n_tp // C
     cap = 5 * tokens // (2 * n_sp)
     slots = n_sp * cap
+    seats = -(-(X * cap // TOP) // 16) * 16
     steps = Y // 2
     msgs = 2 * ring_size(steps)
     part = slots // C // PARTS
@@ -579,10 +617,13 @@
         [pltpu.VMEM(a.shape, a.dtype) for a in operands],
         pltpu.VMEM((Y, C, piece, DV), BF16),
         pltpu.VMEM((128, tokens), F32),
-        pltpu.VMEM((slots, tokens), BF16),
-        pltpu.VMEM((TOP, tokens, slots), BF16),
-        pltpu.VMEM((slots, slots), BF16),
-        pltpu.VMEM((slots, slots), BF16),
+        pltpu.VMEM((8, tokens), F32),
+        pltpu.VMEM((Z * seats, tokens), BF16),
+        pltpu.VMEM((tokens, Z * seats), BF16),
+        pltpu.VMEM((Z, 8, DV), F32),
+        pltpu.VMEM((Z, 8, DV), F32),
+        pltpu.VMEM((slots, Z * seats), BF16),
+        pltpu.VMEM((TOP, Z * seats, slots), BF16),
         pltpu.VMEM(message, BF16),
         pltpu.VMEM((X, *message), BF16),
         pltpu.VMEM(message, BF16),
@@ -590,8 +631,9 @@
         pltpu.VMEM((4, width, hidden), BF16),
         pltpu.VMEM((2, hidden, width), BF16),
         pltpu.VMEM((2, DV, width), BF16),
-        pltpu.VMEM((Y, piece, DV), BF16),
-        pltpu.VMEM((Y, piece, width), F32),
+        pltpu.VMEM((Y, C, piece, DV), BF16),
+        pltpu.VMEM((Y, C * piece, width), F32),
+        pltpu.VMEM((C, piece, width), F32),
         pltpu.VMEM((piece, width), BF16),
         pltpu.VMEM((piece, width), BF16),
         pltpu.VMEM((tokens, DV), BF16),
@@ -600,20 +642,20 @@
         pltpu.VMEM((2, PARTS * part, hidden), BF16),
         pltpu.VMEM((Y, PARTS, part, chunk), F32),
         pltpu.VMEM((PARTS, part, chunk), BF16),
-        pltpu.VMEM((Z, X * cap, DV), BF16),
-        pltpu.VMEM((Z, X * cap, DV), BF16),
+        pltpu.VMEM((Z, seats, DV), BF16),
+        pltpu.VMEM((Z, seats, DV), BF16),
         pltpu.VMEM((X, PARTS // 2, part, DV), BF16),
         pltpu.VMEM((X, PARTS // 2, part, DV), BF16),
-        pltpu.VMEM((Z, X * cap, DV), BF16),
-        pltpu.VMEM((Z, X * cap, DV), BF16),
+        pltpu.VMEM((Z, seats, DV), BF16),
+        pltpu.VMEM((Z, seats, DV), BF16),
         pltpu.VMEM((tokens, DV), BF16),
         pltpu.VMEM((piece, width), BF16),
-        pltpu.VMEM((msgs, piece, width // PARTS), BF16),
-        pltpu.VMEM((msgs, piece, width // PARTS), BF16),
+        pltpu.VMEM((msgs, C * piece, width // PARTS), BF16),
+        pltpu.VMEM((msgs, C * piece, width // PARTS), BF16),
         pltpu.VMEM((msgs, part, chunk), BF16),
         pltpu.VMEM((msgs, part, chunk), BF16),
-        sem((4,)), sem((4,)), sem((4,)), sem((2,)), sem((msgs,)), sem((msgs,)), sem((2,)), sem((2 * C,)),
-        sem((Z,)), sem((Z,)), sem((len(operands),)), sem((10,)), sem((6,)),
+        sem((4,)), sem((4,)), sem((4,)), sem((4,)), sem((msgs,)), sem((msgs,)), sem((2,)), sem((2 * C,)),
+        sem((Z,)), sem((Z,)), sem((len(operands),)), sem((11,)), sem((7,)),
     ]
     return pl.pallas_call(
         functools.partial(layer_kernel, n_sp, n_tp, X, cap),

time: 106 us -> 103 us (0.972)
  Pallas kernels: 105 us -> 102 us
    pallas_call x1, Pallas kernels: 105 us -> 102 us  [shards(): pl.pallas_call(functools.partial(layer_kernel, n_sp, n_tp, X, cap), out_s...]
where the time goes in v4:
time: 103 us
  Pallas kernels  102 us (99%)
    pallas_call x1, Pallas kernels, shards(): pl.pallas_call(functools.partial(layer_kernel, n_sp, n_tp, X, cap), out_s...  102 us

profile of v4, /device:TPU:1, one launch (start us, length us, event | category | flops | bytes accessed | tf_op | source)
XLA Modules:
  0.0 102.9 jit_solution(2589590299127172749)
XLA Ops:
  0.0 102.3 %layer.1 = bf16[16,2048]{1,0:T(8,128)(2,1)S(1)} custom-call(bf16[64,256]{1,0:T(8,128)(2,1)} %bitcast.17, bf16[64,256]{1,0:T(8,128)(2,1)} %bitcast.18, bf16[256,128]{1,0:T(8,128)(2,1)} %operands_2_.1, bf16[256,128]{1,0:T(8,128)(2,1)} %operands_3_.1, bf16[64,256]{1,0:T(8,128)(2,1)} %bitcast.19, f32[1,64]{1,0:T(1,128)} %bitcast.26, f32[1,256]{1,0:T(1,128)} %bitcast.25, ...), custom_call_target="tpu_custom_call" | custom-call | tf_op jit(solution)/shard_map/layer/pallas_call | solution.py:660
  102.3 0.6 copy.20

commit v5 on v4

--- a/solution.py
+++ b/solution.py
@@ -104,8 +104,65 @@
         out(part, total)
 
 
+def relay_sum(at, prepare, part_of, out, sends, recvs, send_sem, recv_sems):
+    Y, y = at.Y, at.y
+    hops = (2, 1, 2, 1)
+    starts = (0, PARTS // 2, PARTS // 2 + PARTS, PARTS // 2 + 2 * PARTS)
+
+    def slot(way, kind, part):
+        return way * ring_size(Y // 2) + starts[kind] + (part % (PARTS // 2) if kind == 0 else part)
+
+    def copy(way, kind, part):
+        i = slot(way, kind, part)
+        to = (y + hops[kind]) % Y if way == 0 else (y + Y - hops[kind]) % Y
+        return remote(sends.at[i], recvs.at[i], send_sem, recv_sems.at[i], at.at(y=to))
+
+    def send(way, kind, part, value):
+        sends[slot(way, kind, part)] = value.astype(BF16)
+        copy(way, kind, part).start()
+
+    def received(way, kind, part):
+        copy(way, kind, part).wait_recv()
+        return recvs[slot(way, kind, part)].astype(F32)
+
+    def own(way, k, part):
+        return part_of(k if way == 0 or k == Y // 2 else -k, part)
+
+    def direct(part):
+        for way in (0, 1):
+            send(way, 3, part, own(way, 1, part))
+
+    for pair in zip(way_parts(0)[0], way_parts(1)[0]):
+        for part in pair:
+            prepare(part)
+            for way in (0, 1):
+                if part in way_parts(way)[0]:
+                    send(way, 0, part, own(way, Y // 2, part))
+                send(way, 1, part, own(way, 3, part))
+    early = way_parts(0)[0]
+    for part in early:
+        direct(part)
+    for way, part in both_ways(lambda w: way_parts(w)[1] + way_parts(w)[0]):
+        value = own(way, 2, part) + received(way, 1, part)
+        if part in way_parts(way)[0]:
+            value = value + received(way, 0, part)
+        send(way, 2, part, value)
+    for part in range(PARTS):
+        if part not in early:
+            direct(part)
+    for part in range(PARTS):
+        total = part_of(0, part)
+        for way in (0, 1):
+            total = total + received(way, 3, part) + received(way, 2, part)
+        out(part, total)
+
+
 def far_first(count):
     return sorted(range(1, count), key=lambda k: (-min(k, count - k), k))
+
+
+def near_order(count):
+    return sorted(range(count), key=lambda k: (min(k, count - k), k))
 
 
 def split(value):
@@ -229,9 +286,17 @@
     before = dot(named, jnp.where(r < q, 1.0, 0.0).astype(BF16))
     targets = []
     plane_of = chosen[0] // X
+    order = near_order(Z)
+    group_size = Z // 2
+    away = z - plane_of
+    away = jnp.where(away < 0, away + Z, away)
+    base = jnp.zeros_like(away)
+    for i, k in enumerate(order):
+        start = (i // group_size) * (X * group_size * cap) + (i % group_size) * cap
+        base = jnp.where(away == k, start, base)
     for e in chosen:
         slot = jnp.sum(jnp.where(sub == e, before, 0.0), axis=0, keepdims=True)
-        targets.append((e - plane_of * X) * (Z * cap) + z * cap + slot.astype(jnp.int32))
+        targets.append((e - plane_of * X) * (group_size * cap) + base + slot.astype(jnp.int32))
     sub = lax.broadcasted_iota(jnp.int32, (Z, tokens), 0)
     before = dot(jnp.where(sub == plane_of, 1.0, 0.0).astype(BF16), jnp.where(r < q, 1.0, 0.0).astype(BF16))
     rank = jnp.sum(jnp.where(sub == plane_of, before, 0.0), axis=0, keepdims=True)
@@ -284,11 +349,13 @@
         told[k] = jnp.where(near, moved[:, 0:DV], 0.0)
 
     def tell(k):
-        return remote(told.at[(z + k) % Z], heard.at[z], done.at[10], came.at[6], at.at(z=(z + k) % Z))
+        return remote(
+            told.at[(z + k) % Z], heard.at[order.index(Z - k)], done.at[10], came.at[6], at.at(z=(z + k) % Z)
+        )
 
     for k in far_first(Z):
         tell(k).start()
-    heard[pl.ds(z, 1)] = told[pl.ds(z, 1)]
+    heard[0:1] = told[pl.ds(z, 1)]
     gate_act = gate_rows[...].astype(F32)
     gate_act = gate_act * jax.nn.sigmoid(gate_act) * head_gain[...]
 
@@ -337,11 +404,13 @@
         swap.wait_recv()
         mine = gated[...].reshape(tokens, DV)
         theirs = partner[...].reshape(tokens, DV)
-        for k in range(PARTS):
-            cols = slice(k * part_width, (k + 1) * part_width)
+
+        def prepare(part):
+            cols = slice(part * part_width, (part + 1) * part_width)
             value = dot(mine, wo[0, :, cols]) + dot(theirs, wo[1, :, cols])
             mixed[:, :, cols] = value.reshape(Y, C * piece, part_width)
-        ring_sum(at, mixed_part, keep, sa, ra, done.at[0], sums)
+
+        relay_sum(at, prepare, mixed_part, keep, sa, ra, done.at[0], sums)
         handed.start()
 
     @pl.when(jnp.logical_not(lead))
@@ -374,7 +443,7 @@
     lax.fori_loop(1, n_tp, start_width, 0)
     block[share_rows(at.tp), :] = normed[:, share_cols(at.tp)]
 
-    whole(heard.at[pl.ds(0, Z - 1)], came.at[6]).wait()
+    whole(heard.at[pl.ds(1, Z - 1)], came.at[6]).wait()
     lists = None
     for k in range(Z):
         part = jnp.concatenate([heard[k], jnp.zeros((8, all_seats - DV), F32)], axis=1)
@@ -394,40 +463,49 @@
     zs[...] = picked.reshape(zs.shape)
 
     def z_out(k):
-        return remote(zs.at[(z + k) % Z], zr.at[z], done.at[5], came.at[2], at.at(z=(z + k) % Z))
-
-    for k in far_first(Z):
-        z_out(k).start()
-    zr[pl.ds(z, 1)] = zs[pl.ds(z, 1)]
-    whole(zr.at[pl.ds(0, Z - 1)], came.at[2]).wait()
-
-    xs[...] = dot(serve[...], zr[...].reshape(all_seats, DV)).astype(BF16).reshape(xs.shape)
+        i = order.index(Z - k)
+        return remote(
+            zs.at[(z + k) % Z], zr.at[i], done.at[5], came.at[2 if i < group_size else 7], at.at(z=(z + k) % Z)
+        )
+
+    for k in order[1:]:
+        z_out(Z - k).start()
+    zr[0:1] = zs[pl.ds(z, 1)]
 
     side = x % C
     mine_half = x // C
     per = PARTS // 2
 
-    def x_out(k):
+    def x_out(half, k):
         to = (x + k) % X
         return (
-            xs.at[to],
-            rows.at[y, pl.ds(mine_half * per, per), :, share_cols(c)],
+            xs.at[half, to],
+            rows.at[y, half * per + mine_half, :, share_cols(c)],
             done.at[8 if k else 9],
-            xrs.at[mine_half],
+            xrs.at[half],
             at.at(x=to, c=side),
         )
 
-    for k in range(1, X):
-        remote(*x_out(k)).start()
-    src, dst, s_sem, r_sem, to = x_out(0)
-
-    @pl.when(side == c)
-    def _():
-        pltpu.make_async_copy(src, dst, r_sem).start()
-
-    @pl.when(side != c)
-    def _():
-        remote(src, dst, s_sem, r_sem, pair).start()
+    for half in (0, 1):
+        first = 1 - half
+        arrived = zr.at[pl.ds(half * group_size + first, group_size - first)]
+        whole(arrived, came.at[7 if half else 2]).wait()
+        listed_rows = slice(half * (slots // 2), (half + 1) * (slots // 2))
+        listed_seats = slice(half * (all_seats // 2), (half + 1) * (all_seats // 2))
+        group_rows = zr[half * group_size : (half + 1) * group_size].reshape(all_seats // 2, DV)
+        picked = dot(serve[listed_rows, listed_seats], group_rows)
+        xs[half] = picked.astype(BF16).reshape(xs.shape[1:])
+        for k in range(1, X):
+            remote(*x_out(half, k)).start()
+        src, dst, s_sem, r_sem, to = x_out(half, 0)
+
+        @pl.when(side == c)
+        def _(src=src, dst=dst, r_sem=r_sem):
+            pltpu.make_async_copy(src, dst, r_sem).start()
+
+        @pl.when(side != c)
+        def _(args=(src, dst, s_sem, r_sem, pair)):
+            remote(*args).start()
 
     def gather(way, step, part):
         j = (y + Y - (step - 1)) % Y if way == 0 else (y + step - 1) % Y
@@ -491,22 +569,20 @@
             made[offset] = True
         return shares[offset + steps - 1, part]
 
-    def x_back(half, core):
-        home = 2 * half + c
+    def x_back(half, column_of, core):
+        home = column_of * C + c
         return (
-            result.at[pl.ds(half * per, per), :, pl.ds(core * DV, DV)],
-            xb.at[x],
-            xbs.at[2 * half + core],
+            result.at[half * per + column_of, :, pl.ds(core * DV, DV)],
+            xb.at[half, x],
+            xbs.at[(half * per + column_of) * C + core],
             came.at[5],
             at.at(x=home, c=core),
         ), (home == x) & (c == core)
 
     def keep_result(part, value):
         result[part] = value.astype(BF16)
-        if part % per < per - 1:
-            return
         for core in range(C):
-            args, here = x_back(part // per, core)
+            args, here = x_back(part // per, part % per, core)
 
             @pl.when(here)
             def _(args=args):
@@ -524,11 +600,11 @@
     zs2[...] = served.astype(BF16).reshape(zs2.shape)
 
     def z_back(k):
-        return remote(zs2.at[(z + k) % Z], zr2.at[z], done.at[6], came.at[3], at.at(z=(z + k) % Z))
+        return remote(zs2.at[order.index(k)], zr2.at[z], done.at[6], came.at[3], at.at(z=(z + k) % Z))
 
     for k in far_first(Z):
         z_back(k).start()
-    zr2[pl.ds(z, 1)] = zs2[pl.ds(z, 1)]
+    zr2[pl.ds(z, 1)] = zs2[0:1]
     whole(zr2.at[pl.ds(0, Z - 1)], came.at[3]).wait()
     column[...] = dot(find[...], zr2[...].reshape(all_seats, DV)).astype(BF16)
 
@@ -574,15 +650,15 @@
     whole(zr.at[pl.ds(0, Z - 1)], done.at[5]).wait()
     whole(told.at[pl.ds(0, Z - 1)], done.at[10]).wait()
     whole(zr2.at[pl.ds(0, Z - 1)], done.at[6]).wait()
-    whole(xs.at[pl.ds(0, X - 1)], done.at[8]).wait()
+    whole(xs.at[:, pl.ds(0, X - 1)], done.at[8]).wait()
 
     @pl.when(side != c)
     def _():
-        remote(src, dst, s_sem, r_sem, pair).wait_send()
-
-    for half in (0, 1):
+        whole(xs.at[:, 0], done.at[9]).wait()
+
+    for part in range(PARTS):
         for core in range(C):
-            args, here = x_back(half, core)
+            args, here = x_back(part // per, part % per, core)
 
             @pl.when(jnp.logical_not(here))
             def _(args=args):
@@ -644,8 +720,8 @@
         pltpu.VMEM((PARTS, part, chunk), BF16),
         pltpu.VMEM((Z, seats, DV), BF16),
         pltpu.VMEM((Z, seats, DV), BF16),
-        pltpu.VMEM((X, PARTS // 2, part, DV), BF16),
-        pltpu.VMEM((X, PARTS // 2, part, DV), BF16),
+        pltpu.VMEM((2, X, part, DV), BF16),
+        pltpu.VMEM((2, X, part, DV), BF16),
         pltpu.VMEM((Z, seats, DV), BF16),
         pltpu.VMEM((Z, seats, DV), BF16),
         pltpu.VMEM((tokens, DV), BF16),
@@ -654,8 +730,8 @@
         pltpu.VMEM((msgs, C * piece, width // PARTS), BF16),
         pltpu.VMEM((msgs, part, chunk), BF16),
         pltpu.VMEM((msgs, part, chunk), BF16),
-        sem((4,)), sem((4,)), sem((4,)), sem((4,)), sem((msgs,)), sem((msgs,)), sem((2,)), sem((2 * C,)),
-        sem((Z,)), sem((Z,)), sem((len(operands),)), sem((11,)), sem((7,)),
+        sem((4,)), sem((4,)), sem((4,)), sem((4,)), sem((msgs,)), sem((msgs,)), sem((2,)), sem((PARTS * C,)),
+        sem((Z,)), sem((Z,)), sem((len(operands),)), sem((11,)), sem((8,)),
     ]
     return pl.pallas_call(
         functools.partial(layer_kernel, n_sp, n_tp, X, cap),

time: 103 us -> 101 us (0.981)
  Pallas kernels: 102 us -> 100 us
    pallas_call x1, Pallas kernels: 102 us -> 100 us  [shards(): pl.pallas_call(functools.partial(layer_kernel, n_sp, n_tp, X, cap), out_s...]
where the time goes in v5:
time: 101 us
  Pallas kernels  100 us (99%)
    pallas_call x1, Pallas kernels, shards(): pl.pallas_call(functools.partial(layer_kernel, n_sp, n_tp, X, cap), out_s...  100 us

profile of v5, /device:TPU:1, one launch (start us, length us, event | category | flops | bytes accessed | tf_op | source)
XLA Modules:
  0.0 100.6 jit_solution(7751783077199099937)
XLA Ops:
  0.0 100.0 %layer.1 = bf16[16,2048]{1,0:T(8,128)(2,1)S(1)} custom-call(bf16[64,256]{1,0:T(8,128)(2,1)} %bitcast.17, bf16[64,256]{1,0:T(8,128)(2,1)} %bitcast.18, bf16[256,128]{1,0:T(8,128)(2,1)} %operands_2_.1, bf16[256,128]{1,0:T(8,128)(2,1)} %operands_3_.1, bf16[64,256]{1,0:T(8,128)(2,1)} %bitcast.19, f32[1,64]{1,0:T(1,128)} %bitcast.26, f32[1,256]{1,0:T(1,128)} %bitcast.25, ...), custom_call_target="tpu_custom_call" | custom-call | tf_op jit(solution)/shard_map/layer/pallas_call | solution.py:736
  100.0 0.6 copy.20

commit v6 on v5

--- a/solution.py
+++ b/solution.py
@@ -186,11 +186,11 @@
 
 def layer_kernel(
     n_sp, n_tp, group, cap,
-    operands, w_out, w_gate, w_up, w_down,
+    operands, residual, w_out, w_gate, w_up, w_down,
     out,
     held,
     gated, stack, facts, spread, find, told, heard, serve, merge, sx, rx, sz, rz,
-    gu, wd, wo, partner, mixed, summed, mid, normed, block, rows, acc, hid, shares, result,
+    gu, wd, wo, partner, mixed, summed, both, mid, normed, block, rows, acc, hid, shares, result,
     zs, zr, xs, xb, zs2, zr2, column, branch,
     sa, ra, sb, rb,
     wsem, wrs, wrr, gsem, sums, gr, xrs, xbs, szs, szr, osem, done, came,
@@ -203,7 +203,7 @@
 
     (
         q_t, k_t, values, gate_rows, decay_t, bias, extra, head_gain,
-        residual, attention_gain, before_gain, after_gain, ids_row, weights_row,
+        attention_gain, before_gain, after_gain, ids_row, weights_row,
     ) = held
     loads = [pltpu.make_async_copy(a, b, osem.at[k]) for k, (a, b) in enumerate(zip(operands, held))]
     for k in loads:
@@ -213,6 +213,7 @@
         pltpu.make_async_copy(w_up, gu.at[1], wsem.at[1]),
         pltpu.make_async_copy(w_down, wd.at[0], wsem.at[2]),
         pltpu.make_async_copy(w_out, wo.at[0], wsem.at[3]),
+        pltpu.make_async_copy(residual, both.at[c], wsem.at[4]),
     ]
     rz[...] = jnp.zeros_like(rz)
     barrier = pltpu.get_barrier_semaphore()
@@ -228,7 +229,7 @@
         for core in range(C):
             pl.semaphore_signal(barrier, inc=1, device_id=at.at(x=(x + k) % X, c=core), device_id_type=MESH)
 
-    for k in (3, 0, 1, 2):
+    for k in (3, 4, 0, 1, 2):
         local[k].start()
     for k in loads:
         k.wait()
@@ -276,6 +277,13 @@
     ]
     for k in crossed:
         k.start()
+    lead = c == C - 1
+    lent = remote(residual, both.at[0], gsem.at[4], gsem.at[5], pair)
+
+    @pl.when(jnp.logical_not(lead))
+    def _():
+        lent.start()
+
     rx[pl.ds(x, 1)] = sx[...].reshape(1, tail, DV)
 
     slots = n_sp * cap
@@ -331,7 +339,7 @@
     def state_z(k):
         return remote(sz, rz.at[z], szs.at[k], szr.at[k], at.at(z=(z + k) % Z))
 
-    for k in range(1, Z):
+    for k in far_first(Z):
 
         @pl.when(z + k < Z)
         def _(k=k):
@@ -377,7 +385,6 @@
     heads = within + jnp.concatenate(across, axis=0)
     heads = heads * lax.rsqrt(jnp.mean(heads * heads, axis=1, keepdims=True) + EPSILON) * gate_act
     gated[...] = heads.astype(BF16).reshape(gated.shape)
-    lead = c == C - 1
     swap = remote(gated, partner, gsem.at[0], gsem.at[1], pair)
 
     @pl.when(jnp.logical_not(lead))
@@ -390,7 +397,7 @@
     local[3].wait()
     crossed[0].wait_recv()
     part_width = width // PARTS
-    handed = remote(summed.at[0], summed.at[0], gsem.at[2], gsem.at[3], pair)
+    handed = remote(mid.at[0], mid.at[0], gsem.at[2], gsem.at[3], pair)
 
     def mixed_part(k, part):
         d = (y + k + Y) % Y
@@ -411,18 +418,15 @@
             mixed[:, :, cols] = value.reshape(Y, C * piece, part_width)
 
         relay_sum(at, prepare, mixed_part, keep, sa, ra, done.at[0], sums)
-        handed.start()
-
-    @pl.when(jnp.logical_not(lead))
-    def _():
-        handed.wait_recv()
-
-    attn = summed[pl.ds(c, 1)].reshape(piece, width)
-    attn = attn * lax.rsqrt(jnp.mean(attn * attn, axis=1, keepdims=True) + EPSILON) * attention_gain[...]
-    mid[...] = (residual[...].astype(F32) + attn).astype(BF16)
-    m = mid[...].astype(F32)
-    m = m * lax.rsqrt(jnp.mean(m * m, axis=1, keepdims=True) + EPSILON) * before_gain[...]
-    normed[...] = m.astype(BF16)
+        lent.wait_recv()
+        local[4].wait()
+        attn = summed[...].reshape(C * piece, width)
+        attn = attn * lax.rsqrt(jnp.mean(attn * attn, axis=1, keepdims=True) + EPSILON) * attention_gain[...]
+        m = (both[...].reshape(C * piece, width).astype(F32) + attn).astype(BF16)
+        mid[...] = m.reshape(C, piece, width)
+        m = m.astype(F32)
+        m = m * lax.rsqrt(jnp.mean(m * m, axis=1, keepdims=True) + EPSILON) * before_gain[...]
+        normed[...] = m.astype(BF16)
 
     def share_cols(t):
         return pl.ds(pl.multiple_of(t * DV, DV), DV)
@@ -430,18 +434,25 @@
     def share_rows(t):
         return pl.ds(pl.multiple_of(t * piece, piece), piece)
 
+    chip_rows = pl.ds(pl.multiple_of(y * (C * piece), C * piece), C * piece)
+
     def to_width(k):
         t = (at.tp + k) % n_tp
-        return remote(
-            normed.at[:, share_cols(t)], block.at[share_rows(at.tp), :], done.at[3], came.at[0], (at.sp, t)
-        )
+        return remote(normed.at[:, share_cols(t)], block.at[chip_rows, :], done.at[3], came.at[0], (at.sp, t))
 
     def start_width(k, carry):
         to_width(k).start()
         return carry
 
-    lax.fori_loop(1, n_tp, start_width, 0)
-    block[share_rows(at.tp), :] = normed[:, share_cols(at.tp)]
+    @pl.when(lead)
+    def _():
+        lax.fori_loop(1, n_tp, start_width, 0)
+        handed.start()
+        block[chip_rows, :] = normed[:, share_cols(at.tp)]
+
+    @pl.when(jnp.logical_not(lead))
+    def _():
+        local[4].wait()
 
     whole(heard.at[pl.ds(1, Z - 1)], came.at[6]).wait()
     lists = None
@@ -458,7 +469,15 @@
         merge[k] = jnp.where(wide == stood[:, k : k + 1].astype(jnp.int32) - 1, 1.0, 0.0).astype(BF16)
     shares_of = [stood[:, TOP + k : TOP + k + 1] for k in range(TOP)]
     others = block.at[pl.ds(0, (n_tp - 1) * piece)]
-    whole(others, came.at[0]).wait()
+
+    @pl.when(lead)
+    def _():
+        whole(block.at[pl.ds(0, (Y - 1) * C * piece)], came.at[0]).wait()
+
+    @pl.when(jnp.logical_not(lead))
+    def _():
+        whole(block, came.at[0]).wait()
+
     picked = dot(spread[...], block[...]).astype(BF16)
     zs[...] = picked.reshape(zs.shape)
 
@@ -623,7 +642,12 @@
     whole(others, came.at[1]).wait()
     b = branch[...].astype(F32)
     b = b * lax.rsqrt(jnp.mean(b * b, axis=1, keepdims=True) + EPSILON) * after_gain[...]
-    out[...] = (mid[...].astype(F32) + b).astype(BF16)
+
+    @pl.when(jnp.logical_not(lead))
+    def _():
+        handed.wait_recv()
+
+    out[...] = (mid[pl.ds(c, 1)].reshape(piece, width).astype(F32) + b).astype(BF16)
 
     whole(rx.at[pl.ds(0, X - 1)], done.at[7]).wait()
     for k in range(1, Z):
@@ -635,17 +659,18 @@
     @pl.when(jnp.logical_not(lead))
     def _():
         swap.wait_send()
+        lent.wait_send()
 
     @pl.when(lead)
     def _():
         handed.wait_send()
+        whole(normed.at[:, pl.ds(0, (n_tp - 1) * DV)], done.at[3]).wait()
         whole(sa, done.at[0]).wait()
 
     for k in crossed:
         k.wait_send()
     whole(sb, done.at[1]).wait()
     whole(rows.at[pl.ds(0, Y - 1)], done.at[2]).wait()
-    whole(others, done.at[3]).wait()
     whole(others, done.at[4]).wait()
     whole(zr.at[pl.ds(0, Z - 1)], done.at[5]).wait()
     whole(told.at[pl.ds(0, Z - 1)], done.at[10]).wait()
@@ -687,7 +712,7 @@
     message = (KEY_CHANNELS + 16, DV)
     operands = [
         query.T, key.T, value, gate_rows, decay.T, bias[None], extra.T, head_gain[None],
-        residual, attention_gain[None], before_gain[None], after_gain[None], ids.T, weights.T,
+        attention_gain[None], before_gain[None], after_gain[None], ids.T, weights.T,
     ]
     scratch = [
         [pltpu.VMEM(a.shape, a.dtype) for a in operands],
@@ -710,8 +735,9 @@
         pltpu.VMEM((Y, C, piece, DV), BF16),
         pltpu.VMEM((Y, C * piece, width), F32),
         pltpu.VMEM((C, piece, width), F32),
-        pltpu.VMEM((piece, width), BF16),
-        pltpu.VMEM((piece, width), BF16),
+        pltpu.VMEM((C, piece, width), BF16),
+        pltpu.VMEM((C, piece, width), BF16),
+        pltpu.VMEM((C * piece, width), BF16),
         pltpu.VMEM((tokens, DV), BF16),
         pltpu.VMEM((Y, PARTS, part, chunk), BF16),
         pltpu.VMEM((4, PARTS * part, hidden), F32),
@@ -730,13 +756,13 @@
         pltpu.VMEM((msgs, C * piece, width // PARTS), BF16),
         pltpu.VMEM((msgs, part, chunk), BF16),
         pltpu.VMEM((msgs, part, chunk), BF16),
-        sem((4,)), sem((4,)), sem((4,)), sem((4,)), sem((msgs,)), sem((msgs,)), sem((2,)), sem((PARTS * C,)),
+        sem((5,)), sem((4,)), sem((4,)), sem((6,)), sem((msgs,)), sem((msgs,)), sem((2,)), sem((PARTS * C,)),
         sem((Z,)), sem((Z,)), sem((len(operands),)), sem((11,)), sem((8,)),
     ]
     return pl.pallas_call(
         functools.partial(layer_kernel, n_sp, n_tp, X, cap),
         out_shape=jax.ShapeDtypeStruct((piece, width), BF16),
-        in_specs=[[hbm] * len(operands), hbm, hbm, hbm, hbm],
+        in_specs=[[hbm] * len(operands), hbm, hbm, hbm, hbm, hbm],
         out_specs=pl.BlockSpec(memory_space=pltpu.VMEM),
         scratch_shapes=scratch,
         name="layer",
@@ -744,7 +770,7 @@
             collective_id=0, has_side_effects=True, vmem_limit_bytes=40 * 1024 * 1024
         ),
     )(
-        *jax.tree.map(lambda a: pltpu.with_memory_space_constraint(a, pltpu.HBM), (operands, output_projection, w_gate[0], w_up[0], w_down[0]))
+        *jax.tree.map(lambda a: pltpu.with_memory_space_constraint(a, pltpu.HBM), (operands, residual, output_projection, w_gate[0], w_up[0], w_down[0]))
     )
 
 

time: 101 us -> 99.6 us (0.986)
  Pallas kernels: 100 us -> 98.8 us
    pallas_call x1, Pallas kernels: 100 us -> 98.8 us  [shards(): pl.pallas_call(functools.partial(layer_kernel, n_sp, n_tp, X, cap), out_s...]
where the time goes in v6:
time: 99.6 us; the launch traced here: 99.5 us
  Pallas kernels  98.8 us (99%)
    pallas_call x1, Pallas kernels, shards(): pl.pallas_call(functools.partial(layer_kernel, n_sp, n_tp, X, cap), out_s...  98.8 us

profile of v6, /device:TPU:1, one launch (start us, length us, event | category | flops | bytes accessed | tf_op | source)
XLA Modules:
  0.0 99.5 jit_solution(13097251557362920216)
XLA Ops:
  0.0 98.8 %layer.1 = bf16[16,2048]{1,0:T(8,128)(2,1)S(1)} custom-call(bf16[64,256]{1,0:T(8,128)(2,1)} %bitcast.17, bf16[64,256]{1,0:T(8,128)(2,1)} %bitcast.18, bf16[256,128]{1,0:T(8,128)(2,1)} %operands_2_.1, bf16[256,128]{1,0:T(8,128)(2,1)} %operands_3_.1, bf16[64,256]{1,0:T(8,128)(2,1)} %bitcast.19, f32[1,64]{1,0:T(1,128)} %bitcast.26, f32[1,256]{1,0:T(1,128)} %bitcast.25, ...), custom_call_target="tpu_custom_call" | custom-call | tf_op jit(solution)/shard_map/layer/pallas_call | solution.py:762
  98.8 0.6 copy.20

commit v7 on v6

--- a/solution.py
+++ b/solution.py
@@ -139,7 +139,7 @@
                 if part in way_parts(way)[0]:
                     send(way, 0, part, own(way, Y // 2, part))
                 send(way, 1, part, own(way, 3, part))
-    early = way_parts(0)[0]
+    early = ()
     for part in early:
         direct(part)
     for way, part in both_ways(lambda w: way_parts(w)[1] + way_parts(w)[0]):
@@ -409,12 +409,11 @@
     @pl.when(lead)
     def _():
         swap.wait_recv()
-        mine = gated[...].reshape(tokens, DV)
-        theirs = partner[...].reshape(tokens, DV)
+        heads_of = jnp.concatenate([gated[...].reshape(tokens, DV), partner[...].reshape(tokens, DV)], axis=1)
 
         def prepare(part):
             cols = slice(part * part_width, (part + 1) * part_width)
-            value = dot(mine, wo[0, :, cols]) + dot(theirs, wo[1, :, cols])
+            value = dot(heads_of, wo[:, :, cols].reshape(2 * DV, part_width))
             mixed[:, :, cols] = value.reshape(Y, C * piece, part_width)
 
         relay_sum(at, prepare, mixed_part, keep, sa, ra, done.at[0], sums)

time: 99.6 us -> 99.3 us (level)
  no operation moved by 1% of the time
where the time goes in v7:
time: 99.3 us; the launch traced here: 99.2 us
  Pallas kernels  98.6 us (99%)
    pallas_call x1, Pallas kernels, shards(): pl.pallas_call(functools.partial(layer_kernel, n_sp, n_tp, X, cap), out_s...  98.6 us

profile of v7, /device:TPU:1, one launch (start us, length us, event | category | flops | bytes accessed | tf_op | source)
XLA Modules:
  0.0 99.2 jit_solution(4158467564688015597)
XLA Ops:
  0.0 98.6 %layer.1 = bf16[16,2048]{1,0:T(8,128)(2,1)S(1)} custom-call(bf16[64,256]{1,0:T(8,128)(2,1)} %bitcast.17, bf16[64,256]{1,0:T(8,128)(2,1)} %bitcast.18, bf16[256,128]{1,0:T(8,128)(2,1)} %operands_2_.1, bf16[256,128]{1,0:T(8,128)(2,1)} %operands_3_.1, bf16[64,256]{1,0:T(8,128)(2,1)} %bitcast.19, f32[1,64]{1,0:T(1,128)} %bitcast.26, f32[1,256]{1,0:T(1,128)} %bitcast.25, ...), custom_call_target="tpu_custom_call" | custom-call | tf_op jit(solution)/shard_map/layer/pallas_call | solution.py:761
  98.6 0.6 copy.20
